TPU v7x, 256 devices: a whole 4x4x8 slice. The times are simulated.
256 devices in a mesh: sp: 32 (over z, y), tp: 8 (over x, core).
Axes of the slice: x: 4, y: 4, z: 8, core: 2. Of those that a mesh axis runs over, the one named last changes fastest.
Arguments:
- activations: bfloat16 [24576, 2048], P(('sp', 'tp')), may hold values from -6 to 6
- in_gain: float32 [2048], replicated, may hold values from 0.1 to 1.9
- w_pool_in: bfloat16 [2048, 1024], P(None, 'tp'), may hold values from -0.125 to 0.125
- pool_gain: float32 [1024], P('tp'), may hold values from 0.1 to 1.9
- w_qlat: bfloat16 [2048, 768], P(None, 'tp'), may hold values from -0.125 to 0.125
- w_kvlat: bfloat16 [2048, 512], P(None, 'tp'), may hold values from -0.125 to 0.125
- w_krope: bfloat16 [2048, 32], replicated, may hold values from -0.125 to 0.125
- qlat_gain: float32 [768], replicated, may hold values from 0.1 to 1.9
- kvlat_gain: float32 [512], replicated, may hold values from 0.1 to 1.9
- w_qup: bfloat16 [768, 1536], P(None, 'tp'), may hold values from -0.21875 to 0.21875
- w_kup: bfloat16 [512, 1024], P(None, 'tp'), may hold values from -0.25 to 0.25
- w_vup: bfloat16 [512, 1024], P(None, 'tp'), may hold values from -0.25 to 0.25
- qhead_gain: float32 [96], replicated, may hold values from 1.1 to 1.9
- khead_gain: float32 [96], replicated, may hold values from 1.1 to 1.9
- w_out_pool: bfloat16 [1024, 2048], P('tp'), may hold values from -0.1875 to 0.1875
- w_out_attn: bfloat16 [1024, 2048], P('tp'), may hold values from -0.75 to 0.75
Outputs:
- mixed: bfloat16 [24576, 2048], P(('sp', 'tp'))
All inputs are finite; a program needn't handle non-finite values.
Results may differ from a plain program's by a relative error of at most 0.025.
Values may be sent and summed in bfloat16 or wider, within the bound.
A program may use at most 128 MiB of HBM per device.

v0:
```python
import math

import jax
import jax.numpy as jnp
from jax import lax
from jax.sharding import PartitionSpec as P

GROUP = 256
NOPE = 64
ROPE = 32
VDIM = 64
QLAT = 768
KVLAT = 512


norm_eps = 1e-06
rope_theta = 10000.0
rim_depth = 15
block_rows = 512


def from_behind(block, axis, distance):
    devices = range(lax.axis_size(axis))
    route = [(i - distance, i) for i in devices if i - distance in devices]
    return lax.ppermute(block, axis, route)


def copy_for_each(x, axis):
    copies = jnp.broadcast_to(x, (lax.axis_size(axis), *x.shape))
    return lax.all_to_all(copies, axis, split_axis=0, concat_axis=0, tiled=True)


def of_everyone(x, axis):
    everything = copy_for_each(x, axis)
    return jnp.sum(everything, axis=0)


def together(arrays, axis):
    ends = [0]
    for a in arrays:
        ends.append(ends[-1] + a.size)
    running = of_everyone(jnp.concatenate([a.ravel() for a in arrays]), axis)
    return tuple((running[b:e].reshape(a.shape) for a, b, e in zip(arrays, ends, ends[1:])))


def side_by_side(arrays, axis, dim, along):
    widths = [a.shape[along] for a in arrays]
    both = jnp.concatenate(arrays, axis=along)
    filled = lax.all_gather(both, axis, axis=dim, tiled=True)
    return tuple(jnp.split(filled, [sum(widths[:k]) for k in range(1, len(widths))], axis=along))


def row_norm(source, norm_gain):
    as_float = source.astype(jnp.float32)
    factor = lax.rsqrt(jnp.mean(as_float * as_float, axis=-1, keepdims=True) + norm_eps)
    return as_float * factor * norm_gain


def rotate(head_rows, positions):
    half_rope = ROPE // 2
    frequency = rope_theta ** (-jnp.arange(0, ROPE, 2, dtype=jnp.float32) / ROPE)
    angles = positions.astype(jnp.float32)[:, None] * frequency[None, :]
    cosine = jnp.cos(angles)[:, None, :]
    sine_part = jnp.sin(angles)[:, None, :]
    plain_part = head_rows[..., :NOPE]
    lower_half = head_rows[..., NOPE : NOPE + half_rope]
    upper_half = head_rows[..., NOPE + half_rope :]
    return jnp.concatenate(
        [
            plain_part,
            lower_half * cosine - upper_half * sine_part,
            upper_half * cosine + lower_half * sine_part,
        ],
        axis=-1,
    )


def pool_mix(extended, positions, channel_start):
    row_count = positions.shape[0]
    width = extended.shape[1]
    channel = channel_start + jnp.arange(width, dtype=jnp.int32)
    window = jnp.left_shift(jnp.int32(2), channel // GROUP)
    as_float = extended.astype(jnp.float32)
    window_sum = jnp.zeros((row_count, width), jnp.float32)
    for lag_index in range(rim_depth + 1):
        lagged = as_float[rim_depth - lag_index : rim_depth - lag_index + row_count]
        window_sum = window_sum + jnp.where(lag_index < window[None, :], lagged, 0.0)
    divisor = jnp.minimum(positions[:, None] + 1, window[None, :]).astype(jnp.float32)
    return window_sum / divisor - as_float[rim_depth:]


def make_queries(q_normed, w_qup, norm_gain, positions):
    row_count = q_normed.shape[0]
    head_count = w_qup.shape[1] // (NOPE + ROPE)
    query_raw = jnp.dot(q_normed, w_qup, preferred_element_type=jnp.float32).astype(jnp.bfloat16)
    query_raw = query_raw.reshape(row_count, head_count, NOPE + ROPE)
    return rotate(row_norm(query_raw, norm_gain), positions).astype(jnp.bfloat16)


def plain_parts(kv_rows, w_kup, w_vup):
    key_plain = jnp.dot(kv_rows, w_kup, preferred_element_type=jnp.float32).astype(jnp.bfloat16)
    value_rows = jnp.dot(kv_rows, w_vup, preferred_element_type=jnp.float32).astype(jnp.bfloat16)
    return (key_plain, value_rows)


def finish_keys(key_plain, rope_rows, norm_gain, positions):
    row_count = key_plain.shape[0]
    head_count = key_plain.shape[1] // NOPE
    key_plain = key_plain.reshape(row_count, head_count, NOPE)
    shared = jnp.broadcast_to(rope_rows[:, None, :], (row_count, head_count, ROPE))
    joined = jnp.concatenate([key_plain, shared], axis=-1)
    key_rows = rotate(row_norm(joined, norm_gain), positions).astype(jnp.bfloat16)
    return key_rows.reshape(row_count, head_count * (NOPE + ROPE))


def update(state_pair, queries, query_pos, key_rows, value_rows, key_pos):
    numerator, denominator = state_pair
    head_count = queries.shape[1]
    key_rows = key_rows.reshape(key_rows.shape[0], head_count, NOPE + ROPE)
    value_rows = value_rows.reshape(value_rows.shape[0], head_count, VDIM)
    scores = jnp.einsum("qhd,khd->hqk", queries, key_rows, preferred_element_type=jnp.float32)
    scores = scores * (NOPE + ROPE) ** (-0.5)
    weights = jnp.where(key_pos[None, None, :] <= query_pos[None, :, None], jnp.exp(scores), 0.0)
    denominator = denominator + jnp.sum(weights, axis=-1)
    numerator = numerator + jnp.einsum(
        "hqk,khd->qhd", weights.astype(jnp.bfloat16), value_rows, preferred_element_type=jnp.float32
    )
    return (numerator, denominator)


def sweep(state_pair, pieces, expand, queries, query_pos):
    shard_rows = queries.shape[0]
    piece_rows = pieces[0].shape[0]
    block_size = shard_rows * math.gcd(piece_rows // shard_rows, max(1, block_rows // shard_rows))

    def advance(block_index, current):
        offset = block_index * block_size

        def accumulate(inner):
            chosen = tuple(
                (lax.dynamic_slice_in_dim(member, offset, block_size, 0) for member in pieces)
            )
            key_pos = offset + jnp.arange(block_size, dtype=jnp.int32)
            key_rows, value_rows = expand(chosen, key_pos)
            return update(inner, queries, query_pos, key_rows, value_rows, key_pos)

        def unchanged(inner):
            return inner

        return lax.cond(offset <= query_pos[-1], accumulate, unchanged, current)

    return lax.fori_loop(0, piece_rows // block_size, advance, state_pair)


def local(
    activations,
    in_gain,
    w_pool_in,
    pool_gain,
    w_qlat,
    w_kvlat,
    w_krope,
    qlat_gain,
    kvlat_gain,
    w_qup,
    w_kup,
    w_vup,
    qhead_gain,
    khead_gain,
    w_out_pool,
    w_out_attn,
):
    own_input = lax.all_gather(activations, "tp", axis=0, tiled=True)
    row_count = own_input.shape[0]
    positions = lax.axis_index("sp") * row_count + jnp.arange(row_count, dtype=jnp.int32)
    normed = row_norm(own_input, in_gain).astype(jnp.bfloat16)
    pool_in = jnp.dot(normed, w_pool_in, preferred_element_type=jnp.float32).astype(jnp.bfloat16)
    prev_rows = from_behind(pool_in[row_count - rim_depth :], "sp", 1)
    extended = jnp.concatenate([prev_rows, pool_in], axis=0)
    channel_start = lax.axis_index("tp") * pool_in.shape[1]
    pool_out = (pool_mix(extended, positions, channel_start) * pool_gain).astype(jnp.bfloat16)
    q_part = jnp.dot(normed, w_qlat, preferred_element_type=jnp.float32).astype(jnp.bfloat16)
    kv_part = jnp.dot(normed, w_kvlat, preferred_element_type=jnp.float32).astype(jnp.bfloat16)
    rope_key = jnp.dot(normed, w_krope, preferred_element_type=jnp.float32).astype(jnp.bfloat16)
    tp_index = lax.axis_index("tp")
    q_width = q_part.shape[1]
    kv_width = kv_part.shape[1]
    q_float = q_part.astype(jnp.float32)
    kv_float = kv_part.astype(jnp.float32)
    q_squares, kv_squares = together(
        (jnp.sum(q_float * q_float, axis=1), jnp.sum(kv_float * kv_float, axis=1)), "tp"
    )
    q_gain = lax.dynamic_slice_in_dim(qlat_gain, tp_index * q_width, q_width)
    kv_gain = lax.dynamic_slice_in_dim(kvlat_gain, tp_index * kv_width, kv_width)
    q_scaled = q_float * lax.rsqrt(q_squares / QLAT + norm_eps)[:, None] * q_gain
    kv_scaled = kv_float * lax.rsqrt(kv_squares / KVLAT + norm_eps)[:, None] * kv_gain
    q_normed, kv_normed = (
        lax.all_gather(q_scaled.astype(jnp.bfloat16), "tp", axis=1, tiled=True),
        lax.all_gather(kv_scaled.astype(jnp.bfloat16), "tp", axis=1, tiled=True),
    )
    queries = make_queries(q_normed, w_qup, qhead_gain, positions)
    head_count = queries.shape[1]
    start_pair = (
        jnp.zeros((row_count, head_count, VDIM), jnp.float32),
        jnp.zeros((head_count, row_count), jnp.float32),
    )
    key_plain, value_rows = plain_parts(kv_normed, w_kup, w_vup)

    def expand_plain(chosen, key_pos):
        return (finish_keys(chosen[0], chosen[2], khead_gain, key_pos), chosen[1])

    numerator, denominator = sweep(
        start_pair,
        side_by_side((key_plain, value_rows, rope_key), "sp", 0, 1),
        expand_plain,
        queries,
        positions,
    )
    attended = (numerator / jnp.transpose(denominator)[:, :, None]).astype(jnp.bfloat16)
    attended = attended.reshape(row_count, head_count * VDIM)
    term = jnp.dot(pool_out, w_out_pool, preferred_element_type=jnp.float32)
    return lax.psum_scatter(
        (term + jnp.dot(attended, w_out_attn, preferred_element_type=jnp.float32)).astype(
            jnp.bfloat16
        ),
        "tp",
        scatter_dimension=0,
        tiled=True,
    )


def solution(mesh):
    placed = (
        P(("sp", "tp"), None),
        P(),
        P(None, "tp"),
        P("tp"),
        P(None, "tp"),
        P(None, "tp"),
        P(),
        P(),
        P(),
        P(None, "tp"),
        P(None, "tp"),
        P(None, "tp"),
        P(),
        P(),
        P("tp", None),
        P("tp", None),
    )
    return jax.shard_map(
        local, mesh=mesh, in_specs=placed, out_specs=P(("sp", "tp"), None), check_vma=False
    )
```

profile of v0, /device:TPU:225, one launch (start us, length us, event | category | flops | bytes accessed | tf_op | source)
XLA Modules:
  0.0 462.3 jit_solution(14622654200361501160)
XLA Ops:
  7.3 33.0 %all-gather.4.cloned.1.call-done = bf16[768,2048]{1,0:T(8,128)(2,1)} async-done(((bf16[96,2048]{1,0:T(8,128)(2,1)}), bf16[768,2048]{1,0:T(8,128)(2,1)}) %all-gather.4.cloned.1.call-update) | async-done | bytes 3145744 | tf_op jit(solution)/shard_map/all_gather | solution.py:173
  40.2 2.7 fusion.23
  43.1 1.5 fusion.25
  47.6 3.5 all-to-all-start
  51.9 4.0 all-to-all-done
  57.5 3.0 convolution_convert_fusion.6
  60.6 14.8 %all_gather.13 = bf16[768,512]{0,1:T(8,128)(2,1)S(1)} all-gather(bf16[768,64]{0,1:T(8,128)(2,1)S(1)} %multiply_convert_fusion.1), channel_id=1, replica_groups=mesh['sp'=32,'tp'=8] {'tp'}, dimensions={1}, use_global_device_ids=true | all-gather | bytes 884736 | tf_op jit(solution)/shard_map/all_gather | solution.py:199
  77.4 2.9 convolution_convert_fusion.1
  80.3 3.3 collective-permute-start
  83.7 3.1 collective-permute-done
  86.9 4.2 fusion.49
  91.1 1.7 convolution_convert_fusion
  93.1 116.8 %all-gather.6.cloned.1.call-done = bf16[24576,288]{0,1:T(8,128)(2,1)} async-done(((bf16[768,288]{0,1:T(8,128)(2,1)}), bf16[24576,288]{0,1:T(8,128)(2,1)}) %all-gather.6.cloned.1.call-update) | async-done | bytes 14155792 | tf_op jit(solution)/shard_map/all_gather | solution.py:49
  209.9 1.5 split.14
  211.4 10.4 %fusion.79 = (bf16[24576,128]{0,1:T(8,128)(2,1)}, bf16[24576,128]{0,1:T(8,128)(2,1)}) fusion(bf16[24576,288]{0,1:T(8,128)(2,1)} %all-gather.6.cloned.1.call-done), kind=kLoop, calls=%fused_computation.156 | loop fusion | bytes 25165824 | tf_op jit(solution)/shard_map/split | solution.py:50
  221.9 181.1 %while.15 = (s32[]{:T(128)}, f32[768,2,64]{0,2,1:T(8,128)S(1)}, f32[2,768]{1,0:T(2,128)S(1)}, s32[768]{0:T(1024)S(1)}, bf16[24576,128]{0,1:T(8,128)(2,1)}, /*ind...) while((s32[]{:T(128)}, f32[768,2,64]{0,2,1:T(8,128)S(1)}, ...), condition=%wide.region_10.11_spmd, body=%wide.region_5.10_spmd.sunk | while | flops 388119616 | bytes 15941421 | solution.py:152
  223.2 4.7 %conditional.2 = ((f32[768,2,64]{0,2,1:T(8,128)S(1)}, f32[2,768]{1,0:T(2,128)S(1)})) conditional(s32[]{:T(128)} %convert_element_type.159, (f32[768,2,64]{0,2,1:T(8,128)S(1)}, f32[2,768]{1,0:T(2,128)S(1)}) %tuple.56, (s32[]{:T(128)}, bf16[24576,128]{0,1:T(8,128)(2,1)}, s32[768]{0:T(1024)S(1)}, bf16[24576,128]{0,1:T(8,128)(2,1)}, ...), branch_computations={%region_6.6_spmd, %region_7.9_spmd} | conditional | flops 388119616 | bytes 15941190 | solution.py:150
  229.3 4.7 %conditional.2 = ((f32[768,2,64]{0,2,1:T(8,128)S(1)}, f32[2,768]{1,0:T(2,128)S(1)})) conditional(s32[]{:T(128)} %convert_element_type.159, (f32[768,2,64]{0,2,1:T(8,128)S(1)}, f32[2,768]{1,0:T(2,128)S(1)}) %tuple.56, (s32[]{:T(128)}, bf16[24576,128]{0,1:T(8,128)(2,1)}, s32[768]{0:T(1024)S(1)}, bf16[24576,128]{0,1:T(8,128)(2,1)}, ...), branch_computations={%region_6.6_spmd, %region_7.9_spmd} | conditional | flops 388119616 | bytes 15941190 | solution.py:150
  235.4 4.7 %conditional.2 = ((f32[768,2,64]{0,2,1:T(8,128)S(1)}, f32[2,768]{1,0:T(2,128)S(1)})) conditional(s32[]{:T(128)} %convert_element_type.159, (f32[768,2,64]{0,2,1:T(8,128)S(1)}, f32[2,768]{1,0:T(2,128)S(1)}) %tuple.56, (s32[]{:T(128)}, bf16[24576,128]{0,1:T(8,128)(2,1)}, s32[768]{0:T(1024)S(1)}, bf16[24576,128]{0,1:T(8,128)(2,1)}, ...), branch_computations={%region_6.6_spmd, %region_7.9_spmd} | conditional | flops 388119616 | bytes 15941190 | solution.py:150
  241.5 4.7 %conditional.2 = ((f32[768,2,64]{0,2,1:T(8,128)S(1)}, f32[2,768]{1,0:T(2,128)S(1)})) conditional(s32[]{:T(128)} %convert_element_type.159, (f32[768,2,64]{0,2,1:T(8,128)S(1)}, f32[2,768]{1,0:T(2,128)S(1)}) %tuple.56, (s32[]{:T(128)}, bf16[24576,128]{0,1:T(8,128)(2,1)}, s32[768]{0:T(1024)S(1)}, bf16[24576,128]{0,1:T(8,128)(2,1)}, ...), branch_computations={%region_6.6_spmd, %region_7.9_spmd} | conditional | flops 388119616 | bytes 15941190 | solution.py:150
  247.6 4.7 %conditional.2 = ((f32[768,2,64]{0,2,1:T(8,128)S(1)}, f32[2,768]{1,0:T(2,128)S(1)})) conditional(s32[]{:T(128)} %convert_element_type.159, (f32[768,2,64]{0,2,1:T(8,128)S(1)}, f32[2,768]{1,0:T(2,128)S(1)}) %tuple.56, (s32[]{:T(128)}, bf16[24576,128]{0,1:T(8,128)(2,1)}, s32[768]{0:T(1024)S(1)}, bf16[24576,128]{0,1:T(8,128)(2,1)}, ...), branch_computations={%region_6.6_spmd, %region_7.9_spmd} | conditional | flops 388119616 | bytes 15941190 | solution.py:150
  253.7 4.7 %conditional.2 = ((f32[768,2,64]{0,2,1:T(8,128)S(1)}, f32[2,768]{1,0:T(2,128)S(1)})) conditional(s32[]{:T(128)} %convert_element_type.159, (f32[768,2,64]{0,2,1:T(8,128)S(1)}, f32[2,768]{1,0:T(2,128)S(1)}) %tuple.56, (s32[]{:T(128)}, bf16[24576,128]{0,1:T(8,128)(2,1)}, s32[768]{0:T(1024)S(1)}, bf16[24576,128]{0,1:T(8,128)(2,1)}, ...), branch_computations={%region_6.6_spmd, %region_7.9_spmd} | conditional | flops 388119616 | bytes 15941190 | solution.py:150
  259.8 4.7 %conditional.2 = ((f32[768,2,64]{0,2,1:T(8,128)S(1)}, f32[2,768]{1,0:T(2,128)S(1)})) conditional(s32[]{:T(128)} %convert_element_type.159, (f32[768,2,64]{0,2,1:T(8,128)S(1)}, f32[2,768]{1,0:T(2,128)S(1)}) %tuple.56, (s32[]{:T(128)}, bf16[24576,128]{0,1:T(8,128)(2,1)}, s32[768]{0:T(1024)S(1)}, bf16[24576,128]{0,1:T(8,128)(2,1)}, ...), branch_computations={%region_6.6_spmd, %region_7.9_spmd} | conditional | flops 388119616 | bytes 15941190 | solution.py:150
  265.9 4.7 %conditional.2 = ((f32[768,2,64]{0,2,1:T(8,128)S(1)}, f32[2,768]{1,0:T(2,128)S(1)})) conditional(s32[]{:T(128)} %convert_element_type.159, (f32[768,2,64]{0,2,1:T(8,128)S(1)}, f32[2,768]{1,0:T(2,128)S(1)}) %tuple.56, (s32[]{:T(128)}, bf16[24576,128]{0,1:T(8,128)(2,1)}, s32[768]{0:T(1024)S(1)}, bf16[24576,128]{0,1:T(8,128)(2,1)}, ...), branch_computations={%region_6.6_spmd, %region_7.9_spmd} | conditional | flops 388119616 | bytes 15941190 | solution.py:150
  272.0 4.7 %conditional.2 = ((f32[768,2,64]{0,2,1:T(8,128)S(1)}, f32[2,768]{1,0:T(2,128)S(1)})) conditional(s32[]{:T(128)} %convert_element_type.159, (f32[768,2,64]{0,2,1:T(8,128)S(1)}, f32[2,768]{1,0:T(2,128)S(1)}) %tuple.56, (s32[]{:T(128)}, bf16[24576,128]{0,1:T(8,128)(2,1)}, s32[768]{0:T(1024)S(1)}, bf16[24576,128]{0,1:T(8,128)(2,1)}, ...), branch_computations={%region_6.6_spmd, %region_7.9_spmd} | conditional | flops 388119616 | bytes 15941190 | solution.py:150
  278.1 4.7 %conditional.2 = ((f32[768,2,64]{0,2,1:T(8,128)S(1)}, f32[2,768]{1,0:T(2,128)S(1)})) conditional(s32[]{:T(128)} %convert_element_type.159, (f32[768,2,64]{0,2,1:T(8,128)S(1)}, f32[2,768]{1,0:T(2,128)S(1)}) %tuple.56, (s32[]{:T(128)}, bf16[24576,128]{0,1:T(8,128)(2,1)}, s32[768]{0:T(1024)S(1)}, bf16[24576,128]{0,1:T(8,128)(2,1)}, ...), branch_computations={%region_6.6_spmd, %region_7.9_spmd} | conditional | flops 388119616 | bytes 15941190 | solution.py:150
  284.2 4.7 %conditional.2 = ((f32[768,2,64]{0,2,1:T(8,128)S(1)}, f32[2,768]{1,0:T(2,128)S(1)})) conditional(s32[]{:T(128)} %convert_element_type.159, (f32[768,2,64]{0,2,1:T(8,128)S(1)}, f32[2,768]{1,0:T(2,128)S(1)}) %tuple.56, (s32[]{:T(128)}, bf16[24576,128]{0,1:T(8,128)(2,1)}, s32[768]{0:T(1024)S(1)}, bf16[24576,128]{0,1:T(8,128)(2,1)}, ...), branch_computations={%region_6.6_spmd, %region_7.9_spmd} | conditional | flops 388119616 | bytes 15941190 | solution.py:150
  290.3 4.7 %conditional.2 = ((f32[768,2,64]{0,2,1:T(8,128)S(1)}, f32[2,768]{1,0:T(2,128)S(1)})) conditional(s32[]{:T(128)} %convert_element_type.159, (f32[768,2,64]{0,2,1:T(8,128)S(1)}, f32[2,768]{1,0:T(2,128)S(1)}) %tuple.56, (s32[]{:T(128)}, bf16[24576,128]{0,1:T(8,128)(2,1)}, s32[768]{0:T(1024)S(1)}, bf16[24576,128]{0,1:T(8,128)(2,1)}, ...), branch_computations={%region_6.6_spmd, %region_7.9_spmd} | conditional | flops 388119616 | bytes 15941190 | solution.py:150
  296.4 4.7 %conditional.2 = ((f32[768,2,64]{0,2,1:T(8,128)S(1)}, f32[2,768]{1,0:T(2,128)S(1)})) conditional(s32[]{:T(128)} %convert_element_type.159, (f32[768,2,64]{0,2,1:T(8,128)S(1)}, f32[2,768]{1,0:T(2,128)S(1)}) %tuple.56, (s32[]{:T(128)}, bf16[24576,128]{0,1:T(8,128)(2,1)}, s32[768]{0:T(1024)S(1)}, bf16[24576,128]{0,1:T(8,128)(2,1)}, ...), branch_computations={%region_6.6_spmd, %region_7.9_spmd} | conditional | flops 388119616 | bytes 15941190 | solution.py:150
  302.5 4.7 %conditional.2 = ((f32[768,2,64]{0,2,1:T(8,128)S(1)}, f32[2,768]{1,0:T(2,128)S(1)})) conditional(s32[]{:T(128)} %convert_element_type.159, (f32[768,2,64]{0,2,1:T(8,128)S(1)}, f32[2,768]{1,0:T(2,128)S(1)}) %tuple.56, (s32[]{:T(128)}, bf16[24576,128]{0,1:T(8,128)(2,1)}, s32[768]{0:T(1024)S(1)}, bf16[24576,128]{0,1:T(8,128)(2,1)}, ...), branch_computations={%region_6.6_spmd, %region_7.9_spmd} | conditional | flops 388119616 | bytes 15941190 | solution.py:150
  308.6 4.7 %conditional.2 = ((f32[768,2,64]{0,2,1:T(8,128)S(1)}, f32[2,768]{1,0:T(2,128)S(1)})) conditional(s32[]{:T(128)} %convert_element_type.159, (f32[768,2,64]{0,2,1:T(8,128)S(1)}, f32[2,768]{1,0:T(2,128)S(1)}) %tuple.56, (s32[]{:T(128)}, bf16[24576,128]{0,1:T(8,128)(2,1)}, s32[768]{0:T(1024)S(1)}, bf16[24576,128]{0,1:T(8,128)(2,1)}, ...), branch_computations={%region_6.6_spmd, %region_7.9_spmd} | conditional | flops 388119616 | bytes 15941190 | solution.py:150
  314.7 4.7 %conditional.2 = ((f32[768,2,64]{0,2,1:T(8,128)S(1)}, f32[2,768]{1,0:T(2,128)S(1)})) conditional(s32[]{:T(128)} %convert_element_type.159, (f32[768,2,64]{0,2,1:T(8,128)S(1)}, f32[2,768]{1,0:T(2,128)S(1)}) %tuple.56, (s32[]{:T(128)}, bf16[24576,128]{0,1:T(8,128)(2,1)}, s32[768]{0:T(1024)S(1)}, bf16[24576,128]{0,1:T(8,128)(2,1)}, ...), branch_computations={%region_6.6_spmd, %region_7.9_spmd} | conditional | flops 388119616 | bytes 15941190 | solution.py:150
  320.9 4.7 %conditional.2 = ((f32[768,2,64]{0,2,1:T(8,128)S(1)}, f32[2,768]{1,0:T(2,128)S(1)})) conditional(s32[]{:T(128)} %convert_element_type.159, (f32[768,2,64]{0,2,1:T(8,128)S(1)}, f32[2,768]{1,0:T(2,128)S(1)}) %tuple.56, (s32[]{:T(128)}, bf16[24576,128]{0,1:T(8,128)(2,1)}, s32[768]{0:T(1024)S(1)}, bf16[24576,128]{0,1:T(8,128)(2,1)}, ...), branch_computations={%region_6.6_spmd, %region_7.9_spmd} | conditional | flops 388119616 | bytes 15941190 | solution.py:150
  326.9 4.7 %conditional.2 = ((f32[768,2,64]{0,2,1:T(8,128)S(1)}, f32[2,768]{1,0:T(2,128)S(1)})) conditional(s32[]{:T(128)} %convert_element_type.159, (f32[768,2,64]{0,2,1:T(8,128)S(1)}, f32[2,768]{1,0:T(2,128)S(1)}) %tuple.56, (s32[]{:T(128)}, bf16[24576,128]{0,1:T(8,128)(2,1)}, s32[768]{0:T(1024)S(1)}, bf16[24576,128]{0,1:T(8,128)(2,1)}, ...), branch_computations={%region_6.6_spmd, %region_7.9_spmd} | conditional | flops 388119616 | bytes 15941190 | solution.py:150
  333.1 4.7 %conditional.2 = ((f32[768,2,64]{0,2,1:T(8,128)S(1)}, f32[2,768]{1,0:T(2,128)S(1)})) conditional(s32[]{:T(128)} %convert_element_type.159, (f32[768,2,64]{0,2,1:T(8,128)S(1)}, f32[2,768]{1,0:T(2,128)S(1)}) %tuple.56, (s32[]{:T(128)}, bf16[24576,128]{0,1:T(8,128)(2,1)}, s32[768]{0:T(1024)S(1)}, bf16[24576,128]{0,1:T(8,128)(2,1)}, ...), branch_computations={%region_6.6_spmd, %region_7.9_spmd} | conditional | flops 388119616 | bytes 15941190 | solution.py:150
  339.2 4.7 %conditional.2 = ((f32[768,2,64]{0,2,1:T(8,128)S(1)}, f32[2,768]{1,0:T(2,128)S(1)})) conditional(s32[]{:T(128)} %convert_element_type.159, (f32[768,2,64]{0,2,1:T(8,128)S(1)}, f32[2,768]{1,0:T(2,128)S(1)}) %tuple.56, (s32[]{:T(128)}, bf16[24576,128]{0,1:T(8,128)(2,1)}, s32[768]{0:T(1024)S(1)}, bf16[24576,128]{0,1:T(8,128)(2,1)}, ...), branch_computations={%region_6.6_spmd, %region_7.9_spmd} | conditional | flops 388119616 | bytes 15941190 | solution.py:150
  345.3 4.7 %conditional.2 = ((f32[768,2,64]{0,2,1:T(8,128)S(1)}, f32[2,768]{1,0:T(2,128)S(1)})) conditional(s32[]{:T(128)} %convert_element_type.159, (f32[768,2,64]{0,2,1:T(8,128)S(1)}, f32[2,768]{1,0:T(2,128)S(1)}) %tuple.56, (s32[]{:T(128)}, bf16[24576,128]{0,1:T(8,128)(2,1)}, s32[768]{0:T(1024)S(1)}, bf16[24576,128]{0,1:T(8,128)(2,1)}, ...), branch_computations={%region_6.6_spmd, %region_7.9_spmd} | conditional | flops 388119616 | bytes 15941190 | solution.py:150
  351.4 4.7 %conditional.2 = ((f32[768,2,64]{0,2,1:T(8,128)S(1)}, f32[2,768]{1,0:T(2,128)S(1)})) conditional(s32[]{:T(128)} %convert_element_type.159, (f32[768,2,64]{0,2,1:T(8,128)S(1)}, f32[2,768]{1,0:T(2,128)S(1)}) %tuple.56, (s32[]{:T(128)}, bf16[24576,128]{0,1:T(8,128)(2,1)}, s32[768]{0:T(1024)S(1)}, bf16[24576,128]{0,1:T(8,128)(2,1)}, ...), branch_computations={%region_6.6_spmd, %region_7.9_spmd} | conditional | flops 388119616 | bytes 15941190 | solution.py:150
  357.5 4.7 %conditional.2 = ((f32[768,2,64]{0,2,1:T(8,128)S(1)}, f32[2,768]{1,0:T(2,128)S(1)})) conditional(s32[]{:T(128)} %convert_element_type.159, (f32[768,2,64]{0,2,1:T(8,128)S(1)}, f32[2,768]{1,0:T(2,128)S(1)}) %tuple.56, (s32[]{:T(128)}, bf16[24576,128]{0,1:T(8,128)(2,1)}, s32[768]{0:T(1024)S(1)}, bf16[24576,128]{0,1:T(8,128)(2,1)}, ...), branch_computations={%region_6.6_spmd, %region_7.9_spmd} | conditional | flops 388119616 | bytes 15941190 | solution.py:150
  363.6 4.7 %conditional.2 = ((f32[768,2,64]{0,2,1:T(8,128)S(1)}, f32[2,768]{1,0:T(2,128)S(1)})) conditional(s32[]{:T(128)} %convert_element_type.159, (f32[768,2,64]{0,2,1:T(8,128)S(1)}, f32[2,768]{1,0:T(2,128)S(1)}) %tuple.56, (s32[]{:T(128)}, bf16[24576,128]{0,1:T(8,128)(2,1)}, s32[768]{0:T(1024)S(1)}, bf16[24576,128]{0,1:T(8,128)(2,1)}, ...), branch_computations={%region_6.6_spmd, %region_7.9_spmd} | conditional | flops 388119616 | bytes 15941190 | solution.py:150
  369.7 4.7 %conditional.2 = ((f32[768,2,64]{0,2,1:T(8,128)S(1)}, f32[2,768]{1,0:T(2,128)S(1)})) conditional(s32[]{:T(128)} %convert_element_type.159, (f32[768,2,64]{0,2,1:T(8,128)S(1)}, f32[2,768]{1,0:T(2,128)S(1)}) %tuple.56, (s32[]{:T(128)}, bf16[24576,128]{0,1:T(8,128)(2,1)}, s32[768]{0:T(1024)S(1)}, bf16[24576,128]{0,1:T(8,128)(2,1)}, ...), branch_computations={%region_6.6_spmd, %region_7.9_spmd} | conditional | flops 388119616 | bytes 15941190 | solution.py:150
  375.8 4.7 %conditional.2 = ((f32[768,2,64]{0,2,1:T(8,128)S(1)}, f32[2,768]{1,0:T(2,128)S(1)})) conditional(s32[]{:T(128)} %convert_element_type.159, (f32[768,2,64]{0,2,1:T(8,128)S(1)}, f32[2,768]{1,0:T(2,128)S(1)}) %tuple.56, (s32[]{:T(128)}, bf16[24576,128]{0,1:T(8,128)(2,1)}, s32[768]{0:T(1024)S(1)}, bf16[24576,128]{0,1:T(8,128)(2,1)}, ...), branch_computations={%region_6.6_spmd, %region_7.9_spmd} | conditional | flops 388119616 | bytes 15941190 | solution.py:150
  381.9 4.7 %conditional.2 = ((f32[768,2,64]{0,2,1:T(8,128)S(1)}, f32[2,768]{1,0:T(2,128)S(1)})) conditional(s32[]{:T(128)} %convert_element_type.159, (f32[768,2,64]{0,2,1:T(8,128)S(1)}, f32[2,768]{1,0:T(2,128)S(1)}) %tuple.56, (s32[]{:T(128)}, bf16[24576,128]{0,1:T(8,128)(2,1)}, s32[768]{0:T(1024)S(1)}, bf16[24576,128]{0,1:T(8,128)(2,1)}, ...), branch_computations={%region_6.6_spmd, %region_7.9_spmd} | conditional | flops 388119616 | bytes 15941190 | solution.py:150
  384.0 1.4 fusion
  388.0 4.7 %conditional.2 = ((f32[768,2,64]{0,2,1:T(8,128)S(1)}, f32[2,768]{1,0:T(2,128)S(1)})) conditional(s32[]{:T(128)} %convert_element_type.159, (f32[768,2,64]{0,2,1:T(8,128)S(1)}, f32[2,768]{1,0:T(2,128)S(1)}) %tuple.56, (s32[]{:T(128)}, bf16[24576,128]{0,1:T(8,128)(2,1)}, s32[768]{0:T(1024)S(1)}, bf16[24576,128]{0,1:T(8,128)(2,1)}, ...), branch_computations={%region_6.6_spmd, %region_7.9_spmd} | conditional | flops 388119616 | bytes 15941190 | solution.py:150
  394.1 4.7 %conditional.2 = ((f32[768,2,64]{0,2,1:T(8,128)S(1)}, f32[2,768]{1,0:T(2,128)S(1)})) conditional(s32[]{:T(128)} %convert_element_type.159, (f32[768,2,64]{0,2,1:T(8,128)S(1)}, f32[2,768]{1,0:T(2,128)S(1)}) %tuple.56, (s32[]{:T(128)}, bf16[24576,128]{0,1:T(8,128)(2,1)}, s32[768]{0:T(1024)S(1)}, bf16[24576,128]{0,1:T(8,128)(2,1)}, ...), branch_computations={%region_6.6_spmd, %region_7.9_spmd} | conditional | flops 388119616 | bytes 15941190 | solution.py:150
  403.0 5.4 %add_convert_fusion.1 = bf16[768,2048]{1,0:T(8,128)(2,1)} fusion(f32[768,2048]{1,0:T(8,128)} %fusion.49, bf16[768,128]{0,1:T(8,128)(2,1)S(1)} %bitcast.48, bf16[128,2048]{1,0:T(8,128)(2,1)S(1)} %copy-done.3), kind=kOutput, calls=%fused_computation.39 | convolution fusion | flops 405798912 | bytes 10158080 | tf_op jit(solution)/shard_map/dot_general | solution.py:223
  408.5 47.3 %reduce-scatter.2.cloned.1.call-done = bf16[96,2048]{1,0:T(8,128)(2,1)} async-done(((bf16[768,2048]{1,0:T(8,128)(2,1)}), bf16[96,2048]{1,0:T(8,128)(2,1)}) %reduce-scatter.2.cloned.1.call-update) | async-done | bytes 393232 | tf_op jit(solution)/shard_map/reduce_scatter | solution.py:222
  (545 shorter events, 162.2 us)
Async XLA Ops:
  6.5 80.3 %copy-start = (bf16[128,2048]{1,0:T(8,128)(2,1)S(1)}, bf16[128,2048]{1,0:T(8,128)(2,1)}, u32[]{:S(2)}) copy-start(bf16[128,2048]{1,0:T(8,128)(2,1)} %param.34) | copy-start | bytes 1572868
  6.5 33.7 %all-gather.4.cloned.1.call-start = ((), (), s32[]{:S(2)}) async-start(), calls=%async_computation.2 | async-start | bytes 3538944 | tf_op jit(solution)/shard_map/all_gather | solution.py:173
  40.2 2.8 copy-start.2
  40.2 4.4 copy-start.6
  43.1 2.7 copy-start.4
  44.6 2.2 copy-start.1
  44.6 12.9 %copy-start.7 = (bf16[2048,32]{0,1:T(8,128)(2,1)S(1)}, bf16[2048,32]{0,1:T(8,128)(2,1)}, u32[]{:S(2)}) copy-start(bf16[2048,32]{0,1:T(8,128)(2,1)} %param.26) | copy-start | bytes 393220
  46.9 28.5 %copy-start.8 = (bf16[512,128]{1,0:T(8,128)(2,1)S(1)}, bf16[512,128]{1,0:T(8,128)(2,1)}, u32[]{:S(2)}) copy-start(bf16[512,128]{1,0:T(8,128)(2,1)} %param.31) | copy-start | bytes 393220
  46.9 28.9 %copy-start.9 = (bf16[512,128]{1,0:T(8,128)(2,1)S(1)}, bf16[512,128]{1,0:T(8,128)(2,1)}, u32[]{:S(2)}) copy-start(bf16[512,128]{1,0:T(8,128)(2,1)} %param.30) | copy-start | bytes 393220
  47.6 8.3 %all-to-all-start = ((f32[8,1,1536]{2,1,0:T(1,128)}), f32[8,1,1536]{2,1,0:T(1,128)S(1)}, u32[]{:S(2)}, u32[]{:S(2)}) async-start(f32[8,1,1536]{2,1,0:T(1,128)} %broadcast_in_dim.188), calls=%async_computation | async-start | bytes 98304 | tf_op jit(solution)/shard_map/all_to_all | solution.py:30
  51.1 40.0 %all-gather.8.cloned.1.call-start = ((), (), s32[]{:S(2)}) async-start(), calls=%async_computation.4 | async-start | bytes 1327104 | tf_op jit(solution)/shard_map/all_gather | solution.py:198
  56.7 153.2 %all-gather.6.cloned.1.call-start = ((), (), s32[]{:S(2)}) async-start(), calls=%async_computation.3 | async-start | bytes 14598144 | tf_op jit(solution)/shard_map/all_gather | solution.py:49
  57.5 19.9 %copy-start.12 = (bf16[2048,128]{1,0:T(8,128)(2,1)S(1)}, bf16[2048,128]{1,0:T(8,128)(2,1)}, u32[]{:S(2)}) copy-start(bf16[2048,128]{1,0:T(8,128)(2,1)} %param.22) | copy-start | bytes 1572868
  75.4 11.4 %copy-start.13 = (f32[128]{0:T(128)S(1)}, f32[128]{0:T(128)}, u32[]{:S(2)}) copy-start(f32[128]{0:T(128)} %param.23) | copy-start | bytes 1540
  76.9 378.9 %reduce-scatter.2.cloned.1.call-start = ((), (), s32[]{:S(2)}) async-start(), calls=%async_computation.5 | async-start | bytes 3538944 | tf_op jit(solution)/shard_map/reduce_scatter | solution.py:222
  80.3 6.5 %collective-permute-start = (bf16[15,128]{1,0:T(8,128)(2,1)S(1)}, bf16[15,128]{1,0:T(8,128)(2,1)S(1)}, u32[]{:S(2)}, u32[]{:S(2)}) collective-permute-start(bf16[15,128]{1,0:T(8,128)(2,1)S(1)} %slice.110), channel_id=1, source_target_pairs={{0,8},{8,16},{16,24},{24,32},{32,40},{40,48},{48,56},{56,64},{64,7... | collective-permute-start | bytes 11528 | tf_op jit(solution)/shard_map/ppermute | solution.py:25
  86.9 4.2 copy-start.5
  86.9 6.0 %copy-start.11 = (f32[96]{0:T(128)S(1)}, f32[96]{0:T(128)}, u32[]{:S(2)}) copy-start(f32[96]{0:T(128)} %param.32) | copy-start | bytes 1156
  211.4 10.4 %copy-start.10 = (f32[96]{0:T(128)S(1)}, f32[96]{0:T(128)}, u32[]{:S(2)}) copy-start(f32[96]{0:T(128)} %param.33) | copy-start | bytes 1156
  221.8 181.2 %copy-start.3 = (bf16[128,2048]{1,0:T(8,128)(2,1)S(1)}, bf16[128,2048]{1,0:T(8,128)(2,1)}, u32[]{:S(2)}) copy-start(bf16[128,2048]{1,0:T(8,128)(2,1)} %param.35) | copy-start | bytes 1572868
Sparse Core Ops, SparseCore 0:
  9.2 31.0 all-gather.3
  56.8 26.6 all-gather.7
  86.1 123.7 all-gather.5
  408.6 47.1 reduce-scatter.1
where the time goes:
time: 469 us; the launch traced here: 462 us
  waiting for transfers between devices  205 us (44%)
  matrix products  95.5 us (20%)
  local copies, waits for them, and re-layouts  67.4 us (14%)
  other arithmetic  33 us (7%)
  loops' own time  26.1 us (6%)
  blocking collectives  14.8 us (3%)
  between operations  13.5 us (3%)
  starting transfers between devices  6.9 us (1%)
    all_gather x1, waiting for transfers between devices, side_by_side(): filled = lax.all_gather(both, axis, axis=dim, tiled=True)  117 us
    reduce_scatter x1, waiting for transfers between devices, local(): lax.psum_scatter((term + jnp.dot(attended, w_out_attn, preferred_element_...  47.3 us
    dot_general x29, matrix products, update(): jnp.einsum('qhd,khd->hqk', queries, key_rows, preferred_element_type=jnp....  39.6 us
    dot_general x29, matrix products, update(): jnp.einsum('hqk,khd->qhd', weights.astype(jnp.bfloat16), value_rows, pref...  36 us
    all_gather x1, waiting for transfers between devices, local(): own_input = lax.all_gather(activations, 'tp', axis=0, tiled=True)  33 us
    dynamic_slice x58, local copies, waits for them, and re-layouts, accumulate(): lax.dynamic_slice_in_dim(member, offset, block_size, 0)  31 us
    another operation x1, loops' own time, sweep(): return lax.fori_loop(0, piece_rows // block_size, advance, state_pair)  23 us
    slice x32, local copies, waits for them, and re-layouts, advance(): return lax.cond(offset <= query_pos[-1], accumulate, unchanged, current)  21.2 us
  transfers between devices with their start and end apart: 6, of which 5 were waited for; matrix products, arithmetic and copies ran while one was open for 3% of the time, Pallas kernels for 0%

commit v1 on v0

v1 whole, which is shorter than its diff:
```python
import functools
import math

import jax
import jax.numpy as jnp
import numpy as np
from jax import lax
from jax.experimental import pallas as pl
from jax.experimental.pallas import tpu as pltpu
from jax.sharding import PartitionSpec as P

NOPE = 64
ROPE = 32
HEAD = NOPE + ROPE
VDIM = 64
QLAT = 768
KVLAT = 512
EPS = 1e-06
THETA = 10000.0
ROWS = 768
BLOCK = 96
HALF = BLOCK // 2
D = 2048
LAT = 160
HALO = 16
F32 = jnp.float32
BF16 = jnp.bfloat16
MESH = pl.DeviceIdType.MESH
VMEM_SPEC = pl.BlockSpec(memory_space=pltpu.VMEM)
SCALE = (1.0 / math.sqrt(HEAD)) * math.log2(math.e)


def dot(a, b):
    return jnp.dot(a, b, preferred_element_type=F32)


def turned(a):
    return jnp.transpose(a.astype(F32))


def rotary_tables():
    freq = THETA ** (-np.arange(0, ROPE, 2, dtype=np.float64) / ROPE)
    far = freq[:, None] * (np.arange(128, dtype=np.float64)[None, :] * ROWS)
    near = freq[:, None] * np.arange(ROWS, dtype=np.float64)[None, :]
    return tuple(t.astype(np.float32) for t in (np.cos(far), np.sin(far), np.cos(near), np.sin(near)))


def place():
    sp = lax.axis_index("sp")
    tp = lax.axis_index("tp")
    return sp, tp, tp // 2, lax.rem(tp, 2)


def meet(devices):
    barrier = pltpu.get_barrier_semaphore()
    for device in devices:
        pl.semaphore_signal(barrier, inc=1, device_id=device, device_id_type=MESH)
    pl.semaphore_wait(barrier, len(devices))


def remote(src, dst, send_sem, recv_sem, device):
    return pltpu.make_async_remote_copy(
        src_ref=src, dst_ref=dst, send_sem=send_sem, recv_sem=recv_sem, device_id=device, device_id_type=MESH
    )


class TpGather:
    def __init__(self, own, everything, half, sp, x, c, ring_send, sib_send, recv):
        self.own, self.all, self.half = own, everything, half
        self.x, self.c = x, c
        self.ring_send, self.sib_send, self.recv = ring_send, sib_send, recv
        self.right = {"sp": sp, "tp": lax.rem(x + 1, 4) * 2 + c}
        self.left = {"sp": sp, "tp": lax.rem(x + 3, 4) * 2 + c}
        self.sib = {"sp": sp, "tp": x * 2 + 1 - c}

    def index(self, offset, core):
        return lax.rem(self.x + 4 + offset, 4) * 2 + core

    def rows(self, h):
        return pl.ds(h * self.half, self.half)

    def piece(self, idx, h):
        return self.all.at[idx, self.rows(h)]

    def copy(self, src, idx, h, send, device):
        return remote(src, self.piece(idx, h), send, self.recv.at[idx, h], device)

    def start(self):
        me = self.index(0, self.c)
        for k, (device, h) in enumerate(((self.right, 0), (self.left, 1), (self.right, 1), (self.left, 0))):
            self.copy(self.own.at[self.rows(h)], me, h, self.ring_send.at[k], device).start()
        for h in range(2):
            self.copy(self.own.at[self.rows(h)], me, h, self.sib_send.at[h], self.sib).start()

    def wait_piece(self, idx, h):
        self.copy(self.own.at[self.rows(h)], idx, h, self.sib_send.at[0], self.sib).wait_recv()

    def got(self, offset, h, slot, onward=None, onward_slot=0):
        idx = self.index(offset, self.c)
        self.wait_piece(idx, h)
        if onward is not None:
            self.copy(self.piece(idx, h), idx, h, self.ring_send.at[onward_slot], onward).start()
        self.copy(self.piece(idx, h), idx, h, self.sib_send.at[slot], self.sib).start()

    def relay_near(self):
        self.got(-1, 0, 2, self.right, 4)
        self.got(1, 1, 3, self.left, 5)
        self.got(-1, 1, 4)
        self.got(1, 0, 5)

    def relay_far(self):
        self.got(2, 0, 6)
        self.got(2, 1, 7)

    def wait_sibling(self, offset):
        idx = self.index(offset, 1 - self.c)
        for h in range(2):
            self.wait_piece(idx, h)
        return idx

    def finish(self):
        for k in range(6):
            self.copy(self.own.at[self.rows(0)], 0, 0, self.ring_send.at[k], self.sib).wait_send()
        for k in range(8):
            self.copy(self.own.at[self.rows(0)], 0, 0, self.sib_send.at[k], self.sib).wait_send()


def front_kernel(
    act, in_gain, w_pool, w_lat, pool_gain, q_gain, kv_gain, w_qup, w_kup, w_vup, qh_gain, kh_gain,
    far_cos, far_sin, near_cos, near_sin,
    q_out, kv_out, pool_out,
    act_all, lat_rows, lat_own, lat_all, pool_rows, halo_out, halo_in, wq_t, wkv_t,
    a_ring, a_sib, a_recv, l_ring, l_sib, l_recv, halo_sem,
):
    sp, tp, x, c = place()
    acts = TpGather(act, act_all, HALF, sp, x, c, a_ring, a_sib, a_recv)
    lats = TpGather(lat_own, lat_all, LAT // 2, sp, x, c, l_ring, l_sib, l_recv)
    behind = {"sp": lax.rem(sp + 1, 32), "tp": tp}
    before = {"sp": lax.rem(sp + 31, 32), "tp": tp}
    meet([acts.right, acts.left, acts.sib, behind, before])
    acts.start()

    def project(block, idx):
        rows = pl.multiple_of(idx * BLOCK, 32)
        value = block[...].astype(F32)
        factor = lax.rsqrt(jnp.mean(value * value, axis=1, keepdims=True) + EPS)
        normed = (value * factor * in_gain[...]).astype(BF16)
        pool_rows[pl.ds(HALO + rows, BLOCK), :] = dot(normed, w_pool[...]).astype(BF16).astype(F32)
        lat_rows[pl.ds(rows, BLOCK), :] = dot(normed, w_lat[...])

    project(act, tp)
    wq_t[...] = turned(w_qup[...]).astype(BF16)
    wkv_t[pl.ds(0, 128), :] = turned(w_kup[...]).astype(BF16)
    wkv_t[pl.ds(128, 128), :] = turned(w_vup[...]).astype(BF16)
    idx = acts.wait_sibling(0)
    project(act_all.at[idx], idx)
    acts.relay_near()
    for offset in (-1, 1):
        idx = acts.index(offset, c)
        project(act_all.at[idx], idx)
    for offset in (-1, 1):
        idx = acts.wait_sibling(offset)
        project(act_all.at[idx], idx)
    acts.relay_far()
    idx = acts.index(2, c)
    project(act_all.at[idx], idx)
    idx = acts.wait_sibling(2)
    project(act_all.at[idx], idx)

    lat_t = jnp.transpose(lat_rows[...])
    lat_own[...] = lat_t[:LAT].astype(BF16)
    rope_t = lat_t[LAT:].astype(BF16).astype(F32)
    halo_out[...] = pool_rows[pl.ds(ROWS, HALO), :].astype(BF16)
    lats.start()
    halo = remote(halo_out, halo_in, halo_sem.at[0], halo_sem.at[1], behind)
    halo.start()
    lat_all[tp] = lat_own[...]

    cos = jnp.sum(jnp.where(lax.broadcasted_iota(jnp.int32, (16, 128), 1) == sp, far_cos[...], 0.0), axis=1, keepdims=True)
    sin = jnp.sum(jnp.where(lax.broadcasted_iota(jnp.int32, (16, 128), 1) == sp, far_sin[...], 0.0), axis=1, keepdims=True)
    cosine = cos * near_cos[...] - sin * near_sin[...]
    sine = sin * near_cos[...] + cos * near_sin[...]

    halo.wait_recv()
    pool_rows[pl.ds(0, HALO), :] = jnp.where(sp > 0, halo_in[...].astype(F32), 0.0)
    window = jnp.left_shift(jnp.int32(2), tp // 2)
    total = jnp.zeros((ROWS, 128), F32)
    for lag in range(16):
        total = total + jnp.where(lag < window, pool_rows[pl.ds(HALO - lag, ROWS), :], 0.0)
    position = sp * ROWS + lax.broadcasted_iota(jnp.int32, (ROWS, 128), 0)
    divisor = jnp.minimum(position + 1, window).astype(F32)
    pooled = total / divisor - pool_rows[pl.ds(HALO, ROWS), :]
    pool_out[...] = (pooled * pool_gain[...]).astype(BF16)

    lats.relay_near()
    lats.relay_far()
    for offset in (0, -1, 1, 2):
        lats.wait_sibling(offset)

    q_lat = lat_all[:, 0:96, :].reshape(QLAT, ROWS).astype(F32)
    q_norm = q_lat * lax.rsqrt(jnp.sum(q_lat * q_lat, axis=0, keepdims=True) / QLAT + EPS) * q_gain[...]
    raw = dot(wq_t[...], q_norm.astype(BF16)).astype(BF16).astype(F32)
    kv_lat = lat_all[:, 96:LAT, :].reshape(KVLAT, ROWS).astype(F32)
    kv_norm = kv_lat * lax.rsqrt(jnp.sum(kv_lat * kv_lat, axis=0, keepdims=True) / KVLAT + EPS) * kv_gain[...]
    plain = dot(wkv_t[...], kv_norm.astype(BF16)).astype(BF16)

    def finish(head, gain):
        factor = lax.rsqrt(jnp.sum(head * head, axis=0, keepdims=True) / HEAD + EPS)
        head = head * factor * gain
        lower, upper = head[64:80], head[80:96]
        return jnp.concatenate([head[:64], lower * cosine - upper * sine, upper * cosine + lower * sine], axis=0)

    for h in range(2):
        q_out[h] = (finish(raw[h * 96 : h * 96 + 96], qh_gain[...]) * SCALE).astype(BF16)
        joined = jnp.concatenate([plain[h * 64 : h * 64 + 64].astype(F32), rope_t], axis=0)
        kv_out[h, 0:96, :] = finish(joined, kh_gain[...]).astype(BF16)
        kv_out[h, 96:160, :] = plain[128 + h * 64 : 192 + h * 64]
    acts.finish()
    lats.finish()
    halo.wait_send()


def attend_kernel(
    q_ref, kv_ref, att_ref,
    kv_all, k_rows, q_in, acc, den, o_stage, att_in,
    c_send, kv_recv, q_send, q_recv, ring_send, sib_send, o_send, o_recv,
):
    sp, tp, x, c = place()
    z, y = sp // 4, lax.rem(sp, 4)

    def device(yy, zz, cc):
        return {"sp": zz * 4 + yy, "tp": x * 2 + cc}

    up = device(y, lax.rem(z + 1, 8), c)
    down = device(y, lax.rem(z + 7, 8), c)
    sib = device(y, z, 1 - c)
    friends = [up, down]
    for dy in range(4):
        for dc in range(2):
            yy, cc = lax.rem(y + dy, 4), lax.rem(c + dc, 2)
            friends.append(device(yy, 7 - z, cc))
            if dy or dc:
                friends.append(device(yy, z, cc))
    meet(friends)

    even = lax.rem(y, 2) == 0
    owner = y // 2
    part = lax.rem(y, 2)

    def kv_copy(j):
        return remote(kv_ref.at[j], kv_all.at[sp], c_send.at[j], kv_recv.at[sp], device(2 * c + j, z, owner))

    def q_copy(j):
        to_z = jnp.where(even, z, 7 - z)
        to_c = jnp.where(even, owner, (3 - y) // 2)
        return remote(q_ref.at[j], q_in.at[part], q_send.at[j], q_recv.at[part], device(2 * c + j, to_z, to_c))

    for j in range(2):
        here = 2 * c + j == y

        @pl.when(jnp.logical_not(here))
        def _():
            kv_copy(j).start()

        @pl.when(here)
        def _():
            kv_all[sp] = kv_ref[j]

    for j in range(2):
        here = jnp.logical_and(even, 2 * c + j == y)

        @pl.when(jnp.logical_not(here))
        def _():
            q_copy(j).start()

        @pl.when(here)
        def _():
            q_in[0] = q_ref[j]

    acc[...] = jnp.zeros_like(acc)
    den[...] = jnp.zeros_like(den)

    def wait_slot(slot):
        remote(kv_all.at[slot], kv_all.at[slot], sib_send.at[slot], kv_recv.at[slot], sib).wait_recv()

    def ring_copy(slot, way, b, s):
        return remote(kv_all.at[slot], kv_all.at[slot], ring_send.at[way, b, s], kv_recv.at[slot], (up, down)[way])

    def sib_copy(slot):
        return remote(kv_all.at[slot], kv_all.at[slot], sib_send.at[slot], kv_recv.at[slot], sib)

    def attend(slot, qb, diagonal):
        for qc in range(3):
            columns = pl.ds(qc * 256, 256)
            keys = (qc + 1) * 256 if diagonal else ROWS
            scores = dot(k_rows[slot, pl.ds(0, keys), :], q_in[qb, :, columns])
            weights = jnp.exp2(scores)
            if diagonal:
                k_pos = lax.broadcasted_iota(jnp.int32, (keys, 256), 0)
                q_pos = lax.broadcasted_iota(jnp.int32, (keys, 256), 1) + qc * 256
                weights = jnp.where(k_pos <= q_pos, weights, 0.0)
            den[qb, :, columns] += jnp.sum(weights.reshape(keys // 8, 8, 256), axis=0)
            acc[qb, :, columns] += dot(kv_all[slot, pl.ds(96, 64), pl.ds(0, keys)], weights.astype(BF16))

    q_index = (z * 4 + 2 * c, (7 - z) * 4 + 3 - 2 * c)

    def plane_of(way, s):
        return lax.rem(z + 8 - s, 8) if way == 0 else lax.rem(z + s, 8)

    @pl.loop(0, 5)
    def _(s):
        for b in range(2):
            @pl.when(jnp.logical_and(s == 0, 2 * c + b != y))
            def _():
                wait_slot(z * 4 + 2 * c + b)

        for b in range(2):
            for way in ((0, 1), (1, 0))[b]:
                limit = 4 if way == b else 3
                slot = plane_of(way, s) * 4 + 2 * c + b

                @pl.when(jnp.logical_and(s >= 1, s <= limit))
                def _():
                    wait_slot(slot)

                @pl.when(s < limit)
                def _():
                    ring_copy(slot, way, b, s).start()

                @pl.when(jnp.logical_and(jnp.logical_or(s >= 1, way == 0), s <= limit))
                def _():
                    sib_copy(slot).start()

        @pl.when(jnp.logical_and(s == 0, 2 * c != y))
        def _():
            remote(q_ref.at[0], q_in.at[0], q_send.at[0], q_recv.at[0], sib).wait_recv()

        @pl.when(s == 0)
        def _():
            remote(q_ref.at[0], q_in.at[1], q_send.at[0], q_recv.at[1], sib).wait_recv()

        planes = jnp.where(jnp.logical_and(s >= 1, s <= 3), 2, 1)

        @pl.loop(0, planes)
        def _(side):
            zb = lax.rem(z + 8 + jnp.where(side == 0, -s, s), 8)
            for b in range(2):
                wait_slot(zb * 4 + 2 * (1 - c) + b)

            @pl.loop(0, 4)
            def _(yb):
                slot = zb * 4 + yb
                needed = slot <= jnp.maximum(q_index[0], q_index[1])

                @pl.when(needed)
                def _():
                    k_rows[slot] = turned(kv_all[slot, pl.ds(0, HEAD), :]).astype(BF16)

                @pl.loop(0, 2)
                def _(qb):
                    query = jnp.where(qb == 0, q_index[0], q_index[1])

                    @pl.when(slot < query)
                    def _():
                        attend(slot, qb, False)

                    @pl.when(slot == query)
                    def _():
                        attend(slot, qb, True)

    def back(qb):
        to_y, to_z = (2 * c, z) if qb == 0 else (3 - 2 * c, 7 - z)
        return remote(o_stage.at[qb], att_in.at[part], o_send.at[qb], o_recv.at[part], device(to_y, to_z, owner))

    for qb in range(2):
        o_stage[qb] = (acc[qb] / jnp.sum(den[qb], axis=0, keepdims=True)).astype(BF16)

    @pl.when(2 * c == y)
    def _():
        att_in[part] = o_stage[0]

    @pl.when(2 * c != y)
    def _():
        back(0).start()

    back(1).start()

    for j in range(2):
        @pl.when(jnp.logical_not(jnp.logical_and(even, 2 * c + j == y)))
        def _():
            remote(o_stage.at[0], att_in.at[j], o_send.at[0], o_recv.at[j], sib).wait_recv()
            q_copy(j).wait_send()

        @pl.when(2 * c + j != y)
        def _():
            kv_copy(j).wait_send()

    att_ref[...] = att_in[...]

    @pl.when(2 * c != y)
    def _():
        back(0).wait_send()

    back(1).wait_send()
    for b in range(2):
        for way in range(2):
            for s in range(4 if way == b else 3):
                ring_copy(0, way, b, s).wait_send()

    @pl.loop(0, 8)
    def _(zb):
        for b in range(2):
            sib_copy(zb * 4 + 2 * c + b).wait_send()


def out_kernel(
    pool_ref, att_ref, w_pool, w_attn, out_ref,
    lhs, w_both, to_sib, from_sib, opp, to_right, to_left, opp_in, from_left, from_right,
    sib_send, sib_recv, opp_send, opp_recv, right_send, right_recv, left_send, left_recv,
):
    sp, tp, x, c = place()
    right = {"sp": sp, "tp": lax.rem(x + 1, 4) * 2 + c}
    left = {"sp": sp, "tp": lax.rem(x + 3, 4) * 2 + c}
    sib = {"sp": sp, "tp": x * 2 + 1 - c}
    meet([right, left, sib])
    w_both[pl.ds(0, 128), :] = w_pool[...]
    w_both[pl.ds(128, 128), :] = w_attn[...]
    lhs[:, 0:128] = pool_ref[...]
    lhs[:, 128:256] = turned(att_ref[...]).astype(BF16)
    order = (2, 1, 3, 0)

    def partial(offset, core):
        rows = pl.multiple_of((lax.rem(x + offset, 4) * 2 + core) * BLOCK, 32)
        return dot(lhs[pl.ds(rows, BLOCK), :], w_both[...])

    def sib_copy(k):
        return remote(to_sib.at[k], from_sib.at[k], sib_send.at[k], sib_recv.at[k], sib)

    for k, offset in enumerate(order):
        to_sib[k] = partial(offset, 1 - c).astype(BF16)
        sib_copy(k).start()

    def chip_sum(k):
        value = partial(order[k], c)
        sib_copy(k).wait_recv()
        return value + from_sib[k].astype(F32)

    first, second = pl.ds(0, HALF), pl.ds(HALF, HALF)
    opp[...] = chip_sum(0).astype(BF16)
    opp_copies = [
        remote(opp.at[first], opp_in.at[0], opp_send.at[0], opp_recv.at[0], right),
        remote(opp.at[second], opp_in.at[1], opp_send.at[1], opp_recv.at[1], left),
    ]
    for copy in opp_copies:
        copy.start()

    def near_copies(stage, landing, send, recv, device):
        return [remote(stage.at[rows], landing.at[rows], send.at[h], recv.at[h], device) for h, rows in enumerate((first, second))]

    rights = near_copies(to_right, from_left, right_send, right_recv, right)
    lefts = near_copies(to_left, from_right, left_send, left_recv, left)
    value_r = chip_sum(1)
    to_right[second, :] = value_r[HALF:].astype(BF16)
    rights[1].start()
    value_l = chip_sum(2)
    to_left[first, :] = value_l[:HALF].astype(BF16)
    lefts[0].start()
    opp_copies[0].wait_recv()
    to_right[first, :] = (value_r[:HALF] + opp_in[0].astype(F32)).astype(BF16)
    rights[0].start()
    opp_copies[1].wait_recv()
    to_left[second, :] = (value_l[HALF:] + opp_in[1].astype(F32)).astype(BF16)
    lefts[1].start()
    value = chip_sum(3)
    for copy in rights + lefts:
        copy.wait_recv()
    out_ref[...] = (value + from_left[...].astype(F32) + from_right[...].astype(F32)).astype(BF16)
    for copy in [sib_copy(k) for k in range(4)] + opp_copies + rights + lefts:
        copy.wait_send()


DMA = pltpu.SemaphoreType.DMA


def params(number):
    return pltpu.CompilerParams(collective_id=number, has_side_effects=True, vmem_limit_bytes=60 * 1024 * 1024)


def local(
    activations, in_gain, w_pool_in, pool_gain, w_qlat, w_kvlat, w_krope, qlat_gain, kvlat_gain,
    w_qup, w_kup, w_vup, qhead_gain, khead_gain, w_out_pool, w_out_attn,
):
    w_lat = jnp.concatenate([w_qlat, w_kvlat, w_krope], axis=1)
    tables = [jnp.asarray(t) for t in rotary_tables()]
    q_t, kv_t, pool_out = pl.pallas_call(
        front_kernel,
        name="front",
        out_shape=(
            jax.ShapeDtypeStruct((2, HEAD, ROWS), BF16),
            jax.ShapeDtypeStruct((2, LAT, ROWS), BF16),
            jax.ShapeDtypeStruct((ROWS, 128), BF16),
        ),
        in_specs=[VMEM_SPEC] * 16,
        out_specs=(VMEM_SPEC,) * 3,
        scratch_shapes=[
            pltpu.VMEM((8, BLOCK, D), BF16),
            pltpu.VMEM((ROWS, 192), F32),
            pltpu.VMEM((LAT, ROWS), BF16),
            pltpu.VMEM((8, LAT, ROWS), BF16),
            pltpu.VMEM((HALO + ROWS, 128), F32),
            pltpu.VMEM((HALO, 128), BF16),
            pltpu.VMEM((HALO, 128), BF16),
            pltpu.VMEM((192, QLAT), BF16),
            pltpu.VMEM((256, KVLAT), BF16),
            DMA((6,)), DMA((8,)), DMA((8, 2)),
            DMA((6,)), DMA((8,)), DMA((8, 2)),
            DMA((2,)),
        ],
        compiler_params=params(1),
    )(
        activations, in_gain[None, :], w_pool_in, w_lat, pool_gain[None, :], qlat_gain[:, None], kvlat_gain[:, None],
        w_qup, w_kup, w_vup, qhead_gain[:, None], khead_gain[:, None], *tables,
    )
    attended = pl.pallas_call(
        attend_kernel,
        name="attend",
        out_shape=jax.ShapeDtypeStruct((2, VDIM, ROWS), BF16),
        in_specs=[VMEM_SPEC] * 2,
        out_specs=VMEM_SPEC,
        scratch_shapes=[
            pltpu.VMEM((32, LAT, ROWS), BF16),
            pltpu.VMEM((32, ROWS, HEAD), BF16),
            pltpu.VMEM((2, HEAD, ROWS), BF16),
            pltpu.VMEM((2, VDIM, ROWS), F32),
            pltpu.VMEM((2, 8, ROWS), F32),
            pltpu.VMEM((2, VDIM, ROWS), BF16),
            pltpu.VMEM((2, VDIM, ROWS), BF16),
            DMA((2,)), DMA((32,)), DMA((2,)), DMA((2,)), DMA((2, 2, 4)), DMA((32,)), DMA((2,)), DMA((2,)),
        ],
        compiler_params=params(2),
    )(q_t, kv_t)
    return pl.pallas_call(
        out_kernel,
        name="output",
        out_shape=jax.ShapeDtypeStruct((BLOCK, D), BF16),
        in_specs=[VMEM_SPEC] * 4,
        out_specs=VMEM_SPEC,
        scratch_shapes=[
            pltpu.VMEM((ROWS, 256), BF16),
            pltpu.VMEM((256, D), BF16),
            pltpu.VMEM((4, BLOCK, D), BF16),
            pltpu.VMEM((4, BLOCK, D), BF16),
            pltpu.VMEM((BLOCK, D), BF16),
            pltpu.VMEM((BLOCK, D), BF16),
            pltpu.VMEM((BLOCK, D), BF16),
            pltpu.VMEM((2, HALF, D), BF16),
            pltpu.VMEM((BLOCK, D), BF16),
            pltpu.VMEM((BLOCK, D), BF16),
            DMA((4,)), DMA((4,)), DMA((2,)), DMA((2,)), DMA((2,)), DMA((2,)), DMA((2,)), DMA((2,)),
        ],
        compiler_params=params(3),
    )(pool_out, attended.reshape(2 * VDIM, ROWS), w_out_pool, w_out_attn)


def solution(mesh):
    placed = (
        P(("sp", "tp"), None), P(), P(None, "tp"), P("tp"), P(None, "tp"), P(None, "tp"), P(), P(), P(),
        P(None, "tp"), P(None, "tp"), P(None, "tp"), P(), P(), P("tp", None), P("tp", None),
    )
    return jax.shard_map(local, mesh=mesh, in_specs=placed, out_specs=P(("sp", "tp"), None), check_vma=False)
```

time: 469 us -> 160 us (0.34)
  the two profiles are of different devices: /device:TPU:225 before, /device:TPU:72 now
where the time goes in v1:
time: 160 us; the launch traced here: 159 us
  Pallas kernels  150 us (94%)
  local copies, waits for them, and re-layouts  7.81 us (5%)
    pallas_call x1, Pallas kernels, local(): pl.pallas_call(attend_kernel, name='attend', out_shape=jax.ShapeDtypeStru...  92.1 us
    pallas_call x1, Pallas kernels, local(): pl.pallas_call(front_kernel, name='front', out_shape=(jax.ShapeDtypeStruc...  36.2 us
    pallas_call x1, Pallas kernels, local(): pl.pallas_call(out_kernel, name='output', out_shape=jax.ShapeDtypeStruct(...  21.6 us
    unnamed x19, local copies, waits for them, and re-layouts  4.58 us

profile of v1, /device:TPU:72, one launch (start us, length us, event | category | flops | bytes accessed | tf_op | source)
XLA Modules:
  0.0 159.4 jit_solution(15335775576590724103)
XLA Ops:
  0.0 0.0 copy-start.1
  0.0 0.0 copy-start.2
  0.0 1.3 copy.27
  1.3 0.0 copy-done.1
  1.3 0.3 copy.28
  1.6 0.0 copy-done.2
  1.6 0.3 copy.29
  1.9 0.0 copy-start.3
  1.9 0.0 copy-start
  1.9 1.6 pad_maximum_fusion.w_lat
  3.5 0.0 copy-done.3
  3.5 0.0 copy-start.4
  3.5 0.0 copy-start.5
  3.5 0.0 copy-start.6
  3.5 0.9 broadcast_in_dim.24.q_gain
  4.4 0.0 copy-done
  4.4 0.9 copy.32.w_qup
  5.4 0.0 copy-done.4
  5.4 0.9 copy.31.kv_gain
  6.2 0.0 copy-done.5
  6.2 0.7 copy.33.qh_gain
  7.0 0.0 copy-done.6
  7.0 0.7 copy.34.kh_gain
  7.7 36.2 %front.1 = (bf16[2,96,768]{2,1,0:T(8,128)(2,1)}, bf16[2,160,768]{2,1,0:T(8,128)(2,1)}, bf16[768,128]{1,0:T(8,128)(2,1)}) custom-call(bf16[96,2048]{1,0:T(8,128)(2,1)} %act.1, f32[1,2048]{1,0:T(1,128)} %bitcast.7, bf16[2048,128]{1,0:T(8,128)(2,1)} %w_pool.2, bf16[2048,192]{1,0:T(8,128)(2,1)} %pad_maximum_fusion.w_lat, f32[1,128]{1,0:T(1,128)} %bitcast.11, ...), custom_call_target="tpu_custom_call" | custom-call | tf_op jit(solution)/shard_map/front/pallas_call | solution.py:495
  43.9 92.1 %attend.1 = bf16[2,64,768]{2,1,0:T(8,128)(2,1)} custom-call(bf16[2,96,768]{2,1,0:T(8,128)(2,1)} %get-tuple-element.9.q_ref, bf16[2,160,768]{2,1,0:T(8,128)(2,1)} %get-tuple-element.10.kv_ref), custom_call_target="tpu_custom_call" | custom-call | tf_op jit(solution)/shard_map/attend/pallas_call | solution.py:524
  135.9 21.6 %output.1 = bf16[96,2048]{1,0:T(8,128)(2,1)} custom-call(bf16[768,128]{1,0:T(8,128)(2,1)} %get-tuple-element.8.pool_ref, bf16[128,768]{1,0:T(8,128)(2,1)} %bitcast.6, bf16[128,2048]{1,0:T(8,128)(2,1)} %w_pool.3, bf16[128,2048]{1,0:T(8,128)(2,1)} %w_attn.1), custom_call_target="tpu_custom_call" | custom-call | tf_op jit(solution)/shard_map/output/pallas_call | solution.py:542
  157.6 1.8 %copy.36 = bf16[96,2048]{1,0:T(8,128)(2,1)} copy(bf16[96,2048]{1,0:T(8,128)(2,1)} %output.1) | data formatting | bytes 786432
Async XLA Ops:
  0.0 1.3 copy-start.1
  0.0 1.6 %copy-start.2 = (bf16[2048,32]{0,1:T(8,128)(2,1)S(1)}, bf16[2048,32]{0,1:T(8,128)(2,1)}, u32[]{:S(2)}) copy-start(bf16[2048,32]{0,1:T(8,128)(2,1)} %param.26) | copy-start | bytes 393220
  1.9 1.6 %copy-start.3 = (f32[768]{0:T(1024)S(1)}, f32[768]{0:T(1024)}, u32[]{:S(2)}) copy-start(f32[768]{0:T(1024)} %param.27) | copy-start | bytes 9220
  1.9 2.5 %copy-start = (bf16[768,192]{0,1:T(8,128)(2,1)S(1)}, bf16[768,192]{0,1:T(8,128)(2,1)}, u32[]{:S(2)}) copy-start(bf16[768,192]{0,1:T(8,128)(2,1)} %param.29) | copy-start | bytes 884740
  3.5 1.8 %copy-start.4 = (f32[512]{0:T(512)S(1)}, f32[512]{0:T(512)}, u32[]{:S(2)}) copy-start(f32[512]{0:T(512)} %param.28) | copy-start | bytes 6148
  3.5 2.7 %copy-start.5 = (f32[96]{0:T(128)S(1)}, f32[96]{0:T(128)}, u32[]{:S(2)}) copy-start(f32[96]{0:T(128)} %param.32) | copy-start | bytes 1156
  3.5 3.4 %copy-start.6 = (f32[96]{0:T(128)S(1)}, f32[96]{0:T(128)}, u32[]{:S(2)}) copy-start(f32[96]{0:T(128)} %param.33) | copy-start | bytes 1156

commit v2 on v1

v2 whole, which is shorter than its diff:
```python
import functools
import math

import jax
import jax.numpy as jnp
import numpy as np
from jax import lax
from jax.experimental import pallas as pl
from jax.experimental.pallas import tpu as pltpu
from jax.sharding import PartitionSpec as P

NOPE = 64
ROPE = 32
HEAD = NOPE + ROPE
VDIM = 64
QLAT = 768
KVLAT = 512
EPS = 1e-06
THETA = 10000.0
ROWS = 768
BLOCK = 96
HALF = BLOCK // 2
D = 2048
LAT = 160
HALO = 16
F32 = jnp.float32
BF16 = jnp.bfloat16
MESH = pl.DeviceIdType.MESH
VMEM_SPEC = pl.BlockSpec(memory_space=pltpu.VMEM)
SCALE = (1.0 / math.sqrt(HEAD)) * math.log2(math.e)


def dot(a, b):
    return jnp.dot(a, b, preferred_element_type=F32)


def turned(a):
    return jnp.transpose(a.astype(F32))


def column(row_ref):
    return jnp.transpose(jnp.broadcast_to(row_ref[...], (8, row_ref.shape[1])))[:, 0:1]


def rotary_tables():
    freq = THETA ** (-np.arange(0, ROPE, 2, dtype=np.float64) / ROPE)
    far = freq[:, None] * (np.arange(128, dtype=np.float64)[None, :] * ROWS)
    near = freq[:, None] * np.arange(ROWS, dtype=np.float64)[None, :]
    return tuple(t.astype(np.float32) for t in (np.cos(far), np.sin(far), np.cos(near), np.sin(near)))


def place():
    sp = lax.axis_index("sp")
    tp = lax.axis_index("tp")
    return sp, tp, tp // 2, lax.rem(tp, 2)


def meet(devices):
    barrier = pltpu.get_barrier_semaphore()
    for device in devices:
        pl.semaphore_signal(barrier, inc=1, device_id=device, device_id_type=MESH)
    pl.semaphore_wait(barrier, len(devices))


def remote(src, dst, send_sem, recv_sem, device):
    return pltpu.make_async_remote_copy(
        src_ref=src, dst_ref=dst, send_sem=send_sem, recv_sem=recv_sem, device_id=device, device_id_type=MESH
    )


class TpGather:
    def __init__(self, own, everything, half, sp, x, c, ring_send, sib_send, recv):
        self.own, self.all, self.half = own, everything, half
        self.x, self.c = x, c
        self.ring_send, self.sib_send, self.recv = ring_send, sib_send, recv
        self.right = {"sp": sp, "tp": lax.rem(x + 1, 4) * 2 + c}
        self.left = {"sp": sp, "tp": lax.rem(x + 3, 4) * 2 + c}
        self.sib = {"sp": sp, "tp": x * 2 + 1 - c}

    def index(self, offset, core):
        return lax.rem(self.x + 4 + offset, 4) * 2 + core

    def piece(self, idx, h):
        return self.all.at[idx, pl.ds(h * self.half, self.half)]

    def copy(self, src, idx, h, send, device):
        return remote(src, self.piece(idx, h), send, self.recv.at[idx, h], device)

    def start(self):
        me = self.index(0, self.c)
        for k, (device, h) in enumerate(((self.right, 0), (self.left, 1), (self.right, 1), (self.left, 0))):
            self.copy(self.own[h], me, h, self.ring_send.at[k], device).start()
        for h in range(2):
            self.copy(self.own[h], me, h, self.sib_send.at[h], self.sib).start()

    def wait_piece(self, idx, h):
        self.copy(self.own[h], idx, h, self.sib_send.at[0], self.sib).wait_recv()

    def got(self, offset, h, slot, onward=None, onward_slot=0):
        idx = self.index(offset, self.c)
        self.wait_piece(idx, h)
        if onward is not None:
            self.copy(self.piece(idx, h), idx, h, self.ring_send.at[onward_slot], onward).start()
        self.copy(self.piece(idx, h), idx, h, self.sib_send.at[slot], self.sib).start()

    def relay_first(self):
        self.got(-1, 0, 2, self.right, 4)
        self.got(1, 1, 3, self.left, 5)

    def relay_second(self):
        self.got(-1, 1, 4)
        self.got(1, 0, 5)

    def relay_far(self):
        self.got(2, 0, 6)
        self.got(2, 1, 7)

    def wait_sibling(self, offset):
        idx = self.index(offset, 1 - self.c)
        for h in range(2):
            self.wait_piece(idx, h)
        return idx

    def finish(self):
        for k in range(6):
            self.copy(self.own[0], 0, 0, self.ring_send.at[k], self.sib).wait_send()
        for k in range(8):
            self.copy(self.own[0], 0, 0, self.sib_send.at[k], self.sib).wait_send()


def front_kernel(
    act, in_gain, w_pool, w_qlat_t, w_kvlat_t, w_krope_t, pool_gain, q_gain, kv_gain, wq_t, w_kup, w_vup, qh_gain, kh_gain,
    far_cos, far_sin, near_cos, near_sin,
    q_out, kv_out, pool_out,
    act_all, lat_rows, lat_own, lat_all, pool_rows, halo_out, halo_in, w_lat, wkv_t,
    a_ring, a_sib, a_recv, l_ring, l_sib, l_recv, halo_sem,
):
    sp, tp, x, c = place()
    acts = TpGather([act.at[pl.ds(0, HALF)], act.at[pl.ds(HALF, HALF)]], act_all, HALF, sp, x, c, a_ring, a_sib, a_recv)
    lats = TpGather([lat_own.at[pl.ds(0, LAT // 2)], lat_own.at[pl.ds(LAT // 2, LAT // 2)]], lat_all, LAT // 2, sp, x, c, l_ring, l_sib, l_recv)
    behind = {"sp": lax.rem(sp + 1, 32), "tp": tp}
    before = {"sp": lax.rem(sp + 31, 32), "tp": tp}
    meet([acts.right, acts.left, acts.sib, behind, before])
    acts.start()

    def project(block, idx):
        rows = pl.multiple_of(idx * BLOCK, 32)
        value = block[...].astype(F32)
        factor = lax.rsqrt(jnp.mean(value * value, axis=1, keepdims=True) + EPS)
        normed = (value * factor * in_gain[...]).astype(BF16)
        pool_rows[pl.ds(HALO + rows, BLOCK), :] = dot(normed, w_pool[...]).astype(BF16).astype(F32)
        lat_rows[pl.ds(rows, BLOCK), :] = dot(normed, w_lat[...])

    w_lat[...] = turned(jnp.concatenate([w_qlat_t[...], w_kvlat_t[...], w_krope_t[...]], axis=0)).astype(BF16)
    project(act, tp)
    wkv_t[pl.ds(0, 128), :] = turned(w_kup[...]).astype(BF16)
    wkv_t[pl.ds(128, 128), :] = turned(w_vup[...]).astype(BF16)
    idx = acts.wait_sibling(0)
    project(act_all.at[idx], idx)
    acts.relay_first()
    acts.relay_second()
    for offset in (-1, 1):
        idx = acts.index(offset, c)
        project(act_all.at[idx], idx)
    for offset in (-1, 1):
        idx = acts.wait_sibling(offset)
        project(act_all.at[idx], idx)
    acts.relay_far()
    idx = acts.index(2, c)
    project(act_all.at[idx], idx)
    idx = acts.wait_sibling(2)
    project(act_all.at[idx], idx)

    lat_t = jnp.transpose(lat_rows[...])
    lat_own[...] = lat_t[:LAT].astype(BF16)
    rope_t = lat_t[LAT:].astype(BF16).astype(F32)
    halo_out[...] = pool_rows[pl.ds(ROWS, HALO), :].astype(BF16)
    lats.start()
    halo = remote(halo_out, halo_in, halo_sem.at[0], halo_sem.at[1], behind)
    halo.start()
    lat_all[tp] = lat_own[...]

    cos = jnp.sum(jnp.where(lax.broadcasted_iota(jnp.int32, (16, 128), 1) == sp, far_cos[...], 0.0), axis=1, keepdims=True)
    sin = jnp.sum(jnp.where(lax.broadcasted_iota(jnp.int32, (16, 128), 1) == sp, far_sin[...], 0.0), axis=1, keepdims=True)
    cosine = cos * near_cos[...] - sin * near_sin[...]
    sine = sin * near_cos[...] + cos * near_sin[...]

    halo.wait_recv()
    pool_rows[pl.ds(0, HALO), :] = jnp.where(sp > 0, halo_in[...].astype(F32), 0.0)
    window = jnp.left_shift(jnp.int32(2), tp // 2)
    total = jnp.zeros((ROWS, 128), F32)
    for lag in range(16):
        total = total + jnp.where(lag < window, pool_rows[pl.ds(HALO - lag, ROWS), :], 0.0)
    position = sp * ROWS + lax.broadcasted_iota(jnp.int32, (ROWS, 128), 0)
    divisor = jnp.minimum(position + 1, window).astype(F32)
    pooled = total / divisor - pool_rows[pl.ds(HALO, ROWS), :]
    pool_out[...] = (pooled * pool_gain[...]).astype(BF16)

    lats.relay_first()
    lats.relay_second()
    lats.relay_far()
    for offset in (0, -1, 1, 2):
        lats.wait_sibling(offset)

    q_lat = lat_all[:, 0:96, :].reshape(QLAT, ROWS).astype(F32)
    q_norm = q_lat * lax.rsqrt(jnp.sum(q_lat * q_lat, axis=0, keepdims=True) / QLAT + EPS) * column(q_gain)
    raw = dot(wq_t[...], q_norm.astype(BF16)).astype(BF16).astype(F32)
    kv_lat = lat_all[:, 96:LAT, :].reshape(KVLAT, ROWS).astype(F32)
    kv_norm = kv_lat * lax.rsqrt(jnp.sum(kv_lat * kv_lat, axis=0, keepdims=True) / KVLAT + EPS) * column(kv_gain)
    plain = dot(wkv_t[...], kv_norm.astype(BF16)).astype(BF16)

    def finish(head, gain):
        factor = lax.rsqrt(jnp.sum(head * head, axis=0, keepdims=True) / HEAD + EPS)
        head = head * factor * gain
        lower, upper = head[64:80], head[80:96]
        return jnp.concatenate([head[:64], lower * cosine - upper * sine, upper * cosine + lower * sine], axis=0)

    for h in range(2):
        q_out[h] = (finish(raw[h * 96 : h * 96 + 96], column(qh_gain)) * SCALE).astype(BF16)
        joined = jnp.concatenate([plain[h * 64 : h * 64 + 64].astype(F32), rope_t], axis=0)
        kv_out[h, 0:96, :] = finish(joined, column(kh_gain)).astype(BF16)
        kv_out[h, 96:160, :] = plain[128 + h * 64 : 192 + h * 64]
    acts.finish()
    lats.finish()
    halo.wait_send()


def attend_kernel(
    q_ref, kv_ref, pool_ref, w_pool, w_attn, out_ref,
    kv_all, k_rows, q_in, acc, den, o_rows, att_all, pool_in, w_all, lhs,
    c_send, kv_recv, q_send, q_recv, ring_send, sib_send, o_send, o_recv, p_send, p_recv, w_ring, w_sib, w_recv,
):
    sp, tp, x, c = place()
    z, y = sp // 4, lax.rem(sp, 4)
    even = lax.rem(y, 2) == 0
    owner = y // 2
    part = lax.rem(y, 2)
    q_z = jnp.where(even, z, 7 - z)
    q_c = jnp.where(even, owner, (3 - y) // 2)

    def device(yy, zz, cc, xx=x):
        return {"sp": zz * 4 + yy, "tp": xx * 2 + cc}

    up = device(y, lax.rem(z + 1, 8), c)
    down = device(y, lax.rem(z + 7, 8), c)
    sib = device(y, z, 1 - c)
    weights_out = TpGather([w_pool, w_attn], w_all, 128, sp, x, c, w_ring, w_sib, w_recv)

    friends = [up, down]
    for dy in range(4):
        for dc in range(2):
            yy, cc = lax.rem(y + dy, 4), lax.rem(c + dc, 2)
            friends.append(device(yy, 7 - z, cc))
            if dy or dc:
                friends.append(device(yy, z, cc))
    friends += [{"sp": sp, "tp": lax.rem(tp + k, 8)} for k in range(1, 8)]
    for dx in range(1, 4):
        for dy in range(4):
            friends.append(device(lax.rem(y + dy, 4), q_z, q_c, lax.rem(x + dx, 4)))
    meet(friends)

    def kv_copy(j):
        return remote(kv_ref.at[j], kv_all.at[sp], c_send.at[j], kv_recv.at[sp], device(2 * c + j, z, owner))

    def q_copy(j):
        return remote(q_ref.at[j], q_in.at[part], q_send.at[j], q_recv.at[part], device(2 * c + j, q_z, q_c))

    for j in range(2):
        here = 2 * c + j == y

        @pl.when(jnp.logical_not(here))
        def _():
            kv_copy(j).start()

        @pl.when(here)
        def _():
            kv_all[sp] = kv_ref[j]

    for j in range(2):
        here = jnp.logical_and(even, 2 * c + j == y)

        @pl.when(jnp.logical_not(here))
        def _():
            q_copy(j).start()

        @pl.when(here)
        def _():
            q_in[0] = q_ref[j]

    weights_out.start()

    def pool_copy(k):
        to = lax.rem(tp + k, 8)
        rows = pl.multiple_of(to * BLOCK, 32)
        return remote(pool_ref.at[pl.ds(rows, BLOCK)], pool_in.at[tp], p_send.at[k], p_recv.at[tp], {"sp": sp, "tp": to})

    for k in range(1, 8):
        pool_copy(k).start()
    pool_in[tp] = pool_ref[pl.ds(pl.multiple_of(tp * BLOCK, 32), BLOCK), :]
    w_all[tp, pl.ds(0, 128), :] = w_pool[...]
    w_all[tp, pl.ds(128, 128), :] = w_attn[...]
    acc[...] = jnp.zeros_like(acc)
    den[...] = jnp.zeros_like(den)

    def wait_slot(slot):
        remote(kv_all.at[slot], kv_all.at[slot], sib_send.at[slot], kv_recv.at[slot], sib).wait_recv()

    def ring_copy(slot, way, b, s):
        return remote(kv_all.at[slot], kv_all.at[slot], ring_send.at[way, b, s], kv_recv.at[slot], (up, down)[way])

    def sib_copy(slot):
        return remote(kv_all.at[slot], kv_all.at[slot], sib_send.at[slot], kv_recv.at[slot], sib)

    def attend(slots, qb, diagonal):
        for qc in range(3):
            columns = pl.ds(qc * 256, 256)
            keys = (qc + 1) * 256 if diagonal else ROWS
            for slot in slots:
                scores = dot(k_rows[slot, pl.ds(0, keys), :], q_in[qb, :, columns])
                weights = jnp.exp2(scores)
                if diagonal:
                    k_pos = lax.broadcasted_iota(jnp.int32, (keys, 256), 0)
                    q_pos = lax.broadcasted_iota(jnp.int32, (keys, 256), 1) + qc * 256
                    weights = jnp.where(k_pos <= q_pos, weights, 0.0)
                den[qb, :, columns] += jnp.sum(weights.reshape(keys // 8, 8, 256), axis=0)
                acc[qb, :, columns] += dot(kv_all[slot, pl.ds(96, 64), pl.ds(0, keys)], weights.astype(BF16))

    q_plane = (z, 7 - z)
    q_row = (2 * c, 3 - 2 * c)

    def plane_of(way, s):
        return lax.rem(z + 8 - s, 8) if way == 0 else lax.rem(z + s, 8)

    def pass_on(s, b):
        @pl.when(jnp.logical_and(s == 0, 2 * c + b != y))
        def _():
            wait_slot(z * 4 + 2 * c + b)

        for way in ((0, 1), (1, 0))[b]:
            limit = 4 if way == b else 3
            slot = plane_of(way, s) * 4 + 2 * c + b

            @pl.when(jnp.logical_and(s >= 1, s <= limit))
            def _():
                wait_slot(slot)

            @pl.when(s < limit)
            def _():
                ring_copy(slot, way, b, s).start()

            @pl.when(jnp.logical_and(jnp.logical_or(s >= 1, way == 0), s <= limit))
            def _():
                sib_copy(slot).start()

    def use(zb):
        first = zb * 4
        for b in range(2):
            wait_slot(first + 2 * (1 - c) + b)

        @pl.when(zb <= jnp.maximum(z, 7 - z))
        def _():
            for yb in range(4):
                k_rows[first + yb] = turned(kv_all[first + yb, pl.ds(0, HEAD), :]).astype(BF16)

        @pl.loop(0, 2)
        def _(qb):
            plane = jnp.where(qb == 0, q_plane[0], q_plane[1])
            row = jnp.where(qb == 0, q_row[0], q_row[1])

            @pl.when(zb < plane)
            def _():
                attend([first + yb for yb in range(4)], qb, False)

            @pl.when(zb == plane)
            def _():
                @pl.loop(0, row)
                def _(yb):
                    attend([first + yb], qb, False)

                attend([first + row], qb, True)

    @pl.loop(0, 10)
    def _(turn):
        s, b = turn // 2, lax.rem(turn, 2)
        for k in range(2):
            @pl.when(b == k)
            def _():
                pass_on(s, k)

        @pl.when(jnp.logical_and(turn == 1, 2 * c != y))
        def _():
            remote(q_ref.at[0], q_in.at[0], q_send.at[0], q_recv.at[0], sib).wait_recv()

        @pl.when(turn == 1)
        def _():
            remote(q_ref.at[0], q_in.at[1], q_send.at[0], q_recv.at[1], sib).wait_recv()

        @pl.when(turn == 4)
        def _():
            weights_out.relay_first()

        @pl.when(turn == 6)
        def _():
            weights_out.relay_second()

        @pl.when(turn == 8)
        def _():
            weights_out.relay_far()

        done = s - 1
        zb = lax.rem(z + 8 + jnp.where(b == 0, -done, done), 8)

        @pl.when(jnp.logical_and(turn >= 2, turn != 3))
        def _():
            use(zb)

    use(lax.rem(z + 4, 8))

    def back(qb, t):
        to_y, to_z = (2 * c, z) if qb == 0 else (3 - 2 * c, 7 - z)
        return remote(
            o_rows.at[qb, pl.ds(t * BLOCK, BLOCK)], att_all.at[4 * x + y], o_send.at[qb, t], o_recv.at[4 * x + y],
            {"sp": to_z * 4 + to_y, "tp": t},
        )

    mine = jnp.logical_and(even, 2 * c == y)

    def is_me(qb, t):
        return jnp.logical_and(2 * c == y, tp == t) if qb == 0 else False

    for qb in (1, 0):
        o_rows[qb] = jnp.transpose(acc[qb] / jnp.sum(den[qb], axis=0, keepdims=True)).astype(BF16)
        for t in range(8):
            if qb == 1:
                back(qb, t).start()
            else:
                @pl.when(jnp.logical_not(is_me(qb, t)))
                def _():
                    back(qb, t).start()

                @pl.when(is_me(qb, t))
                def _():
                    att_all[4 * x + y] = o_rows[0, pl.ds(t * BLOCK, BLOCK), :]

    for k in range(1, 8):
        idx = lax.rem(tp + k, 8)
        remote(pool_in.at[0], pool_in.at[idx], p_send.at[k], p_recv.at[idx], sib).wait_recv()
    for offset in (0, -1, 1, 2):
        weights_out.wait_sibling(offset)
    for t in range(8):
        lhs[:, pl.ds(t * 256, 128)] = pool_in[t]

    @pl.loop(0, 16)
    def _(head):
        @pl.when(jnp.logical_not(jnp.logical_and(mine, head == 4 * x + y)))
        def _():
            remote(att_all.at[0], att_all.at[head], o_send.at[0, 0], o_recv.at[head], sib).wait_recv()

    for t in range(8):
        lhs[:, pl.ds(t * 256 + 128, 128)] = jnp.concatenate([att_all[2 * t], att_all[2 * t + 1]], axis=1)
    for part_of in range(4):
        columns = pl.ds(part_of * 512, 512)
        out_ref[:, columns] = dot(lhs[...], w_all[:, :, columns].reshape(D, 512)).astype(BF16)

    for j in range(2):
        @pl.when(jnp.logical_not(jnp.logical_and(even, 2 * c + j == y)))
        def _():
            q_copy(j).wait_send()

        @pl.when(2 * c + j != y)
        def _():
            kv_copy(j).wait_send()

    for t in range(8):
        back(1, t).wait_send()

        @pl.when(jnp.logical_not(is_me(0, t)))
        def _():
            back(0, t).wait_send()

    for k in range(1, 8):
        pool_copy(k).wait_send()
    weights_out.finish()
    for b in range(2):
        for way in range(2):
            for s in range(4 if way == b else 3):
                ring_copy(0, way, b, s).wait_send()

    @pl.loop(0, 8)
    def _(zb):
        for b in range(2):
            sib_copy(zb * 4 + 2 * c + b).wait_send()


DMA = pltpu.SemaphoreType.DMA


def params(number):
    return pltpu.CompilerParams(collective_id=number, has_side_effects=True, vmem_limit_bytes=60 * 1024 * 1024)


def local(
    activations, in_gain, w_pool_in, pool_gain, w_qlat, w_kvlat, w_krope, qlat_gain, kvlat_gain,
    w_qup, w_kup, w_vup, qhead_gain, khead_gain, w_out_pool, w_out_attn,
):
    tables = [jnp.asarray(t) for t in rotary_tables()]
    q_t, kv_t, pool_out = pl.pallas_call(
        front_kernel,
        name="front",
        out_shape=(
            jax.ShapeDtypeStruct((2, HEAD, ROWS), BF16),
            jax.ShapeDtypeStruct((2, LAT, ROWS), BF16),
            jax.ShapeDtypeStruct((ROWS, 128), BF16),
        ),
        in_specs=[VMEM_SPEC] * 18,
        out_specs=(VMEM_SPEC,) * 3,
        scratch_shapes=[
            pltpu.VMEM((8, BLOCK, D), BF16),
            pltpu.VMEM((ROWS, 192), F32),
            pltpu.VMEM((LAT, ROWS), BF16),
            pltpu.VMEM((8, LAT, ROWS), BF16),
            pltpu.VMEM((HALO + ROWS, 128), F32),
            pltpu.VMEM((HALO, 128), BF16),
            pltpu.VMEM((HALO, 128), BF16),
            pltpu.VMEM((D, 192), BF16),
            pltpu.VMEM((256, KVLAT), BF16),
            DMA((6,)), DMA((8,)), DMA((8, 2)),
            DMA((6,)), DMA((8,)), DMA((8, 2)),
            DMA((2,)),
        ],
        compiler_params=params(1),
    )(
        activations, in_gain[None, :], w_pool_in, w_qlat.T, w_kvlat.T, w_krope.T, pool_gain[None, :], qlat_gain[None, :],
        kvlat_gain[None, :], w_qup.T, w_kup, w_vup, qhead_gain[None, :], khead_gain[None, :], *tables,
    )
    return pl.pallas_call(
        attend_kernel,
        name="attend",
        out_shape=jax.ShapeDtypeStruct((BLOCK, D), BF16),
        in_specs=[VMEM_SPEC] * 5,
        out_specs=VMEM_SPEC,
        scratch_shapes=[
            pltpu.VMEM((32, LAT, ROWS), BF16),
            pltpu.VMEM((32, ROWS, HEAD), BF16),
            pltpu.VMEM((2, HEAD, ROWS), BF16),
            pltpu.VMEM((2, VDIM, ROWS), F32),
            pltpu.VMEM((2, 8, ROWS), F32),
            pltpu.VMEM((2, ROWS, VDIM), BF16),
            pltpu.VMEM((16, BLOCK, VDIM), BF16),
            pltpu.VMEM((8, BLOCK, 128), BF16),
            pltpu.VMEM((8, 256, D), BF16),
            pltpu.VMEM((BLOCK, D), BF16),
            DMA((2,)), DMA((32,)), DMA((2,)), DMA((2,)), DMA((2, 2, 4)), DMA((32,)), DMA((2, 8)), DMA((16,)),
            DMA((8,)), DMA((8,)), DMA((6,)), DMA((8,)), DMA((8, 2)),
        ],
        compiler_params=params(2),
    )(q_t, kv_t, pool_out, w_out_pool, w_out_attn)


def solution(mesh):
    placed = (
        P(("sp", "tp"), None), P(), P(None, "tp"), P("tp"), P(None, "tp"), P(None, "tp"), P(), P(), P(),
        P(None, "tp"), P(None, "tp"), P(None, "tp"), P(), P(), P("tp", None), P("tp", None),
    )
    return jax.shard_map(local, mesh=mesh, in_specs=placed, out_specs=P(("sp", "tp"), None), check_vma=False)
```

time: 160 us -> 128 us (0.80)
  the two profiles are of different devices: /device:TPU:72 before, /device:TPU:111 now
where the time goes in v2:
time: 128 us; the launch traced here: 127 us
  Pallas kernels  124 us (97%)
  local copies, waits for them, and re-layouts  3.03 us (2%)
    pallas_call x1, Pallas kernels, local(): pl.pallas_call(attend_kernel, name='attend', out_shape=jax.ShapeDtypeStru...  89.2 us
    pallas_call x1, Pallas kernels, local(): pl.pallas_call(front_kernel, name='front', out_shape=(jax.ShapeDtypeStruc...  35.2 us

profile of v2, /device:TPU:111, one launch (start us, length us, event | category | flops | bytes accessed | tf_op | source)
XLA Modules:
  0.0 127.5 jit_solution(17207411803810767906)
XLA Ops:
  0.0 0.0 copy-start
  0.0 0.7 copy-done
  0.7 0.6 broadcast_in_dim.20.q_gain
  1.3 35.2 %front.1 = (bf16[2,96,768]{2,1,0:T(8,128)(2,1)}, bf16[2,160,768]{2,1,0:T(8,128)(2,1)}, bf16[768,128]{1,0:T(8,128)(2,1)}) custom-call(bf16[96,2048]{1,0:T(8,128)(2,1)} %act.1, f32[1,2048]{1,0:T(1,128)} %bitcast.13, bf16[2048,128]{1,0:T(8,128)(2,1)} %w_pool.2, bf16[96,2048]{1,0:T(8,128)(2,1)} %bitcast.9, bf16[64,2048]{1,0:T(8,128)(2,1)} %bitcast.11, ...), custom_call_target="tpu_custom_call" | custom-call | tf_op jit(solution)/shard_map/front/pallas_call | solution.py:507
  36.5 89.2 %attend.1 = bf16[96,2048]{1,0:T(8,128)(2,1)} custom-call(bf16[2,96,768]{2,1,0:T(8,128)(2,1)} %get-tuple-element.8.q_ref, bf16[2,160,768]{2,1,0:T(8,128)(2,1)} %get-tuple-element.9.kv_ref, bf16[768,128]{1,0:T(8,128)(2,1)} %get-tuple-element.10.pool_ref, bf16[128,2048]{1,0:T(8,128)(2,1)} %w_pool.3, bf16[128,2048]{1,0:T(8,128)(2,1)} %w_attn.1), custom_call_target="tpu_custom_call" | custom-call | tf_op jit(solution)/shard_map/attend/pallas_call | solution.py:536
  125.7 1.8 %copy.22 = bf16[96,2048]{1,0:T(8,128)(2,1)} copy(bf16[96,2048]{1,0:T(8,128)(2,1)} %attend.1) | data formatting | bytes 786432
Async XLA Ops:
  0.0 0.7 copy-start

commit v3 on v2

v3 whole, which is shorter than its diff:
```python
import functools
import math

import jax
import jax.numpy as jnp
import numpy as np
from jax import lax
from jax.experimental import pallas as pl
from jax.experimental.pallas import tpu as pltpu
from jax.sharding import PartitionSpec as P

NOPE = 64
ROPE = 32
HEAD = NOPE + ROPE
VDIM = 64
QLAT = 768
KVLAT = 512
EPS = 1e-06
THETA = 10000.0
ROWS = 768
BLOCK = 96
HALF = BLOCK // 2
D = 2048
LAT = 160
HALO = 16
F32 = jnp.float32
BF16 = jnp.bfloat16
MESH = pl.DeviceIdType.MESH
VMEM_SPEC = pl.BlockSpec(memory_space=pltpu.VMEM)
SCALE = (1.0 / math.sqrt(HEAD)) * math.log2(math.e)


def dot(a, b):
    return jnp.dot(a, b, preferred_element_type=F32)


def turned(a):
    return jnp.transpose(a.astype(F32))


def column(row_ref):
    return jnp.transpose(jnp.broadcast_to(row_ref[...], (8, row_ref.shape[1])))[:, 0:1]


def rotary_tables():
    freq = THETA ** (-np.arange(0, ROPE, 2, dtype=np.float64) / ROPE)
    far = freq[:, None] * (np.arange(128, dtype=np.float64)[None, :] * ROWS)
    near = freq[:, None] * np.arange(ROWS, dtype=np.float64)[None, :]
    return tuple(t.astype(np.float32) for t in (np.cos(far), np.sin(far), np.cos(near), np.sin(near)))


def place():
    sp = lax.axis_index("sp")
    tp = lax.axis_index("tp")
    return sp, tp, tp // 2, lax.rem(tp, 2)


def meet(devices):
    barrier = pltpu.get_barrier_semaphore()
    for device in devices:
        pl.semaphore_signal(barrier, inc=1, device_id=device, device_id_type=MESH)
    pl.semaphore_wait(barrier, len(devices))


def remote(src, dst, send_sem, recv_sem, device):
    return pltpu.make_async_remote_copy(
        src_ref=src, dst_ref=dst, send_sem=send_sem, recv_sem=recv_sem, device_id=device, device_id_type=MESH
    )


class TpGather:
    def __init__(self, own, everything, half, sp, x, c, ring_send, sib_send, recv):
        self.own, self.all, self.half = own, everything, half
        self.x, self.c = x, c
        self.ring_send, self.sib_send, self.recv = ring_send, sib_send, recv
        self.right = {"sp": sp, "tp": lax.rem(x + 1, 4) * 2 + c}
        self.left = {"sp": sp, "tp": lax.rem(x + 3, 4) * 2 + c}
        self.sib = {"sp": sp, "tp": x * 2 + 1 - c}

    def index(self, offset, core):
        return lax.rem(self.x + 4 + offset, 4) * 2 + core

    def piece(self, idx, h):
        return self.all.at[idx, pl.ds(h * self.half, self.half)]

    def copy(self, src, idx, h, send, device):
        return remote(src, self.piece(idx, h), send, self.recv.at[idx, h], device)

    def start(self):
        me = self.index(0, self.c)
        for k, (device, h) in enumerate(((self.right, 0), (self.left, 1), (self.right, 1), (self.left, 0))):
            self.copy(self.own[h], me, h, self.ring_send.at[k], device).start()
        for h in range(2):
            self.copy(self.own[h], me, h, self.sib_send.at[h], self.sib).start()

    def wait_piece(self, idx, h):
        self.copy(self.own[h], idx, h, self.sib_send.at[0], self.sib).wait_recv()

    def got(self, offset, h, slot, onward=None, onward_slot=0):
        idx = self.index(offset, self.c)
        self.wait_piece(idx, h)
        if onward is not None:
            self.copy(self.piece(idx, h), idx, h, self.ring_send.at[onward_slot], onward).start()
        self.copy(self.piece(idx, h), idx, h, self.sib_send.at[slot], self.sib).start()

    def relay_first(self):
        self.got(-1, 0, 2, self.right, 4)
        self.got(1, 1, 3, self.left, 5)

    def relay_second(self):
        self.got(-1, 1, 4)
        self.got(1, 0, 5)

    def relay_far(self):
        self.got(2, 0, 6)
        self.got(2, 1, 7)

    def wait_sibling(self, offset):
        idx = self.index(offset, 1 - self.c)
        for h in range(2):
            self.wait_piece(idx, h)
        return idx

    def finish(self):
        for k in range(6):
            self.copy(self.own[0], 0, 0, self.ring_send.at[k], self.sib).wait_send()
        for k in range(8):
            self.copy(self.own[0], 0, 0, self.sib_send.at[k], self.sib).wait_send()


def mixer_kernel(
    act, in_gain, w_pool, w_qlat_t, w_kvlat_t, w_krope_t, pool_gain, q_gain, kv_gain, wq_t, w_kup, w_vup, qh_gain, kh_gain,
    far_cos, far_sin, near_cos, near_sin, w_out_pool, w_out_attn,
    out_ref,
    act_all, lat_rows, kvl_own, kvl_all, ql_own, ql_all, pool_rows, halo_out, halo_in, w_lat, wkv_t, q_own, kv_own, pool_own,
    kv_all, k_rows, q_in, acc, den, o_rows, att_all, pool_in, w_all, lhs, total,
    a_ring, a_sib, a_recv, k_ring, k_sib, k_recv, l_ring, l_sib, l_recv, halo_sem,
    c_send, kv_recv, q_send, q_recv, ring_send, sib_send, o_send, o_recv, p_send, p_recv, w_ring, w_sib, w_recv,
):
    sp, tp, x, c = place()
    z, y = sp // 4, lax.rem(sp, 4)
    even = lax.rem(y, 2) == 0
    owner = y // 2
    part = lax.rem(y, 2)
    q_z = jnp.where(even, z, 7 - z)
    q_c = jnp.where(even, owner, (3 - y) // 2)

    def device(yy, zz, cc, xx=x):
        return {"sp": zz * 4 + yy, "tp": xx * 2 + cc}

    up = device(y, lax.rem(z + 1, 8), c)
    down = device(y, lax.rem(z + 7, 8), c)
    sib = device(y, z, 1 - c)
    behind = {"sp": lax.rem(sp + 1, 32), "tp": tp}
    before = {"sp": lax.rem(sp + 31, 32), "tp": tp}

    def gather(own, everything, half, *sems):
        return TpGather(own, everything, half, sp, x, c, *sems)

    acts = gather([act.at[pl.ds(0, HALF)], act.at[pl.ds(HALF, HALF)]], act_all, HALF, a_ring, a_sib, a_recv)
    kv_lats = gather([kvl_own.at[pl.ds(0, 32)], kvl_own.at[pl.ds(32, 32)]], kvl_all, 32, k_ring, k_sib, k_recv)
    q_lats = gather([ql_own.at[pl.ds(0, 48)], ql_own.at[pl.ds(48, 48)]], ql_all, 48, l_ring, l_sib, l_recv)
    weights_out = gather([w_out_pool, w_out_attn], w_all, 128, w_ring, w_sib, w_recv)

    friends = [up, down, behind, before]
    for dy in range(4):
        for dc in range(2):
            yy, cc = lax.rem(y + dy, 4), lax.rem(c + dc, 2)
            friends.append(device(yy, 7 - z, cc))
            if dy or dc:
                friends.append(device(yy, z, cc))
    friends += [{"sp": sp, "tp": lax.rem(tp + k, 8)} for k in range(1, 8)]
    for dx in range(1, 4):
        for dy in range(4):
            friends.append(device(lax.rem(y + dy, 4), q_z, q_c, lax.rem(x + dx, 4)))
    meet(friends)

    acts.start()

    def project(block, idx):
        rows = pl.multiple_of(idx * BLOCK, 32)
        value = block[...].astype(F32)
        factor = lax.rsqrt(jnp.mean(value * value, axis=1, keepdims=True) + EPS)
        normed = (value * factor * in_gain[...]).astype(BF16)
        pool_rows[pl.ds(HALO + rows, BLOCK), :] = dot(normed, w_pool[...]).astype(BF16).astype(F32)
        lat_rows[pl.ds(rows, BLOCK), :] = dot(normed, w_lat[...])

    w_lat[...] = turned(jnp.concatenate([w_qlat_t[...], w_kvlat_t[...], w_krope_t[...]], axis=0)).astype(BF16)
    project(act, tp)
    wkv_t[pl.ds(0, 128), :] = turned(w_kup[...]).astype(BF16)
    wkv_t[pl.ds(128, 128), :] = turned(w_vup[...]).astype(BF16)
    idx = acts.wait_sibling(0)
    project(act_all.at[idx], idx)
    acts.relay_first()
    acts.relay_second()
    for offset in (-1, 1):
        idx = acts.index(offset, c)
        project(act_all.at[idx], idx)
    for offset in (-1, 1):
        idx = acts.wait_sibling(offset)
        project(act_all.at[idx], idx)
    acts.relay_far()
    idx = acts.index(2, c)
    project(act_all.at[idx], idx)
    idx = acts.wait_sibling(2)
    project(act_all.at[idx], idx)

    lat_t = jnp.transpose(lat_rows[...])
    kvl_own[...] = lat_t[96:160].astype(BF16)
    ql_own[...] = lat_t[0:96].astype(BF16)
    rope_t = lat_t[160:192].astype(BF16).astype(F32)
    halo_out[...] = pool_rows[pl.ds(ROWS, HALO), :].astype(BF16)
    kv_lats.start()
    halo = remote(halo_out, halo_in, halo_sem.at[0], halo_sem.at[1], behind)
    halo.start()
    kvl_all[tp] = kvl_own[...]
    ql_all[tp] = ql_own[...]

    column_of = lax.broadcasted_iota(jnp.int32, (16, 128), 1) == sp
    cos = jnp.sum(jnp.where(column_of, far_cos[...], 0.0), axis=1, keepdims=True)
    sin = jnp.sum(jnp.where(column_of, far_sin[...], 0.0), axis=1, keepdims=True)
    cosine = cos * near_cos[...] - sin * near_sin[...]
    sine = sin * near_cos[...] + cos * near_sin[...]

    kv_lats.relay_first()
    q_lats.start()
    kv_lats.relay_second()
    kv_lats.relay_far()
    for offset in (0, -1, 1, 2):
        kv_lats.wait_sibling(offset)

    def finish(head, gain):
        factor = lax.rsqrt(jnp.sum(head * head, axis=0, keepdims=True) / HEAD + EPS)
        head = head * factor * gain
        lower, upper = head[64:80], head[80:96]
        return jnp.concatenate([head[:64], lower * cosine - upper * sine, upper * cosine + lower * sine], axis=0)

    kv_lat = kvl_all[...].reshape(KVLAT, ROWS).astype(F32)
    kv_norm = kv_lat * lax.rsqrt(jnp.sum(kv_lat * kv_lat, axis=0, keepdims=True) / KVLAT + EPS) * column(kv_gain)
    plain = dot(wkv_t[...], kv_norm.astype(BF16)).astype(BF16)
    for h in range(2):
        joined = jnp.concatenate([plain[h * 64 : h * 64 + 64].astype(F32), rope_t], axis=0)
        kv_own[h, 0:96, :] = finish(joined, column(kh_gain)).astype(BF16)
        kv_own[h, 96:160, :] = plain[128 + h * 64 : 192 + h * 64]

    def kv_copy(j):
        return remote(kv_own.at[j], kv_all.at[sp], c_send.at[j], kv_recv.at[sp], device(2 * c + j, z, owner))

    def q_copy(j):
        return remote(q_own.at[j], q_in.at[part], q_send.at[j], q_recv.at[part], device(2 * c + j, q_z, q_c))

    for j in range(2):
        here = 2 * c + j == y

        @pl.when(jnp.logical_not(here))
        def _():
            kv_copy(j).start()

        @pl.when(here)
        def _():
            kv_all[sp] = kv_own[j]

    q_lats.relay_first()
    q_lats.relay_second()
    q_lats.relay_far()
    for offset in (0, -1, 1, 2):
        q_lats.wait_sibling(offset)
    weights_out.start()
    q_lat = ql_all[...].reshape(QLAT, ROWS).astype(F32)
    q_norm = q_lat * lax.rsqrt(jnp.sum(q_lat * q_lat, axis=0, keepdims=True) / QLAT + EPS) * column(q_gain)
    raw = dot(wq_t[...], q_norm.astype(BF16)).astype(BF16).astype(F32)
    for h in range(2):
        q_own[h] = (finish(raw[h * 96 : h * 96 + 96], column(qh_gain)) * SCALE).astype(BF16)

    for j in range(2):
        here = jnp.logical_and(even, 2 * c + j == y)

        @pl.when(jnp.logical_not(here))
        def _():
            q_copy(j).start()

        @pl.when(here)
        def _():
            q_in[0] = q_own[j]

    def wait_slot(slot):
        remote(kv_all.at[slot], kv_all.at[slot], sib_send.at[slot], kv_recv.at[slot], sib).wait_recv()

    def ring_copy(slot, way, b, s):
        return remote(kv_all.at[slot], kv_all.at[slot], ring_send.at[way, b, s], kv_recv.at[slot], (up, down)[way])

    def sib_copy(slot):
        return remote(kv_all.at[slot], kv_all.at[slot], sib_send.at[slot], kv_recv.at[slot], sib)

    def pool_copy(k):
        to = lax.rem(tp + k, 8)
        rows = pl.multiple_of(to * BLOCK, 32)
        return remote(pool_own.at[pl.ds(rows, BLOCK)], pool_in.at[tp], p_send.at[k], p_recv.at[tp], {"sp": sp, "tp": to})

    def mix_pool():
        halo.wait_recv()
        pool_rows[pl.ds(0, HALO), :] = jnp.where(sp > 0, halo_in[...].astype(F32), 0.0)
        window = jnp.left_shift(jnp.int32(2), tp // 2)
        summed = jnp.zeros((ROWS, 128), F32)
        for lag in range(16):
            summed = summed + jnp.where(lag < window, pool_rows[pl.ds(HALO - lag, ROWS), :], 0.0)
        position = sp * ROWS + lax.broadcasted_iota(jnp.int32, (ROWS, 128), 0)
        divisor = jnp.minimum(position + 1, window).astype(F32)
        pooled = summed / divisor - pool_rows[pl.ds(HALO, ROWS), :]
        pool_own[...] = (pooled * pool_gain[...]).astype(BF16)
        for k in range(1, 8):
            pool_copy(k).start()
        pool_in[tp] = pool_own[pl.ds(pl.multiple_of(tp * BLOCK, 32), BLOCK), :]
        w_all[tp, pl.ds(0, 128), :] = w_out_pool[...]
        w_all[tp, pl.ds(128, 128), :] = w_out_attn[...]
        acc[...] = jnp.zeros_like(acc)
        den[...] = jnp.zeros_like(den)

    def attend(slots, qb, diagonal):
        for qc in range(3):
            columns = pl.ds(qc * 256, 256)
            keys = (qc + 1) * 256 if diagonal else ROWS
            for slot in slots:
                scores = dot(k_rows[slot, pl.ds(0, keys), :], q_in[qb, :, columns])
                weights = jnp.exp2(scores)
                if diagonal:
                    k_pos = lax.broadcasted_iota(jnp.int32, (keys, 256), 0)
                    q_pos = lax.broadcasted_iota(jnp.int32, (keys, 256), 1) + qc * 256
                    weights = jnp.where(k_pos <= q_pos, weights, 0.0)
                den[qb, :, columns] += jnp.sum(weights.reshape(keys // 8, 8, 256), axis=0)
                acc[qb, :, columns] += dot(kv_all[slot, pl.ds(96, 64), pl.ds(0, keys)], weights.astype(BF16))

    def plane_of(way, s):
        return lax.rem(z + 8 - s, 8) if way == 0 else lax.rem(z + s, 8)

    def pass_on(s, b):
        @pl.when(jnp.logical_and(s == 0, 2 * c + b != y))
        def _():
            wait_slot(z * 4 + 2 * c + b)

        for way in ((0, 1), (1, 0))[b]:
            limit = 4 if way == b else 3
            slot = plane_of(way, s) * 4 + 2 * c + b

            @pl.when(jnp.logical_and(s >= 1, s <= limit))
            def _():
                wait_slot(slot)

            @pl.when(s < limit)
            def _():
                ring_copy(slot, way, b, s).start()

            @pl.when(jnp.logical_and(jnp.logical_or(s >= 1, way == 0), s <= limit))
            def _():
                sib_copy(slot).start()

    def query_block(qb):
        return jnp.where(qb == 0, z, 7 - z), jnp.where(qb == 0, 2 * c, 3 - 2 * c)

    def unpack(zb):
        first = zb * 4
        for b in range(2):
            wait_slot(first + 2 * (1 - c) + b)

        @pl.when(zb <= jnp.maximum(z, 7 - z))
        def _():
            for yb in range(4):
                k_rows[first + yb] = turned(kv_all[first + yb, pl.ds(0, HEAD), :]).astype(BF16)

    def use(zb, qb):
        first = zb * 4
        plane, row = query_block(qb)

        @pl.when(zb < plane)
        def _():
            attend([first + yb for yb in range(4)], qb, False)

        @pl.when(zb == plane)
        def _():
            @pl.loop(0, row)
            def _(yb):
                attend([first + yb], qb, False)

            attend([first + row], qb, True)

    def back(qb, t):
        to_z, to_y = query_block(qb)
        return remote(
            o_rows.at[qb, t], att_all.at[4 * x + y], o_send.at[qb, t], o_recv.at[4 * x + y],
            {"sp": to_z * 4 + to_y, "tp": t},
        )

    def is_me(qb, t):
        return jnp.logical_and(jnp.logical_and(qb == 0, 2 * c == y), tp == t)

    def send_back(qb):
        rows = jnp.transpose(acc[qb] / jnp.sum(den[qb], axis=0, keepdims=True)).reshape(8, 2, HALF, VDIM)
        o_rows[qb] = jnp.concatenate([rows[:, 0], rows[:, 1]], axis=2).astype(BF16)
        for t in range(8):
            @pl.when(jnp.logical_not(is_me(qb, t)))
            def _():
                back(qb, t).start()

            @pl.when(is_me(qb, t))
            def _():
                att_all[4 * x + y] = o_rows[qb, t]

    @pl.loop(0, 11)
    def _(turn):
        s, b = turn // 2, lax.rem(turn, 2)
        for k in range(2):
            @pl.when(jnp.logical_and(b == k, turn < 10))
            def _():
                pass_on(s, k)

        @pl.when(turn == 1)
        def _():
            mix_pool()

        @pl.when(jnp.logical_and(turn == 1, 2 * c != y))
        def _():
            remote(q_own.at[0], q_in.at[0], q_send.at[0], q_recv.at[0], sib).wait_recv()

        @pl.when(turn == 1)
        def _():
            remote(q_own.at[0], q_in.at[1], q_send.at[0], q_recv.at[1], sib).wait_recv()

        @pl.when(turn == 4)
        def _():
            weights_out.relay_first()

        @pl.when(turn == 6)
        def _():
            weights_out.relay_second()

        @pl.when(turn == 8)
        def _():
            weights_out.relay_far()

        done = s - 1
        zb = lax.rem(z + 8 + jnp.where(b == 0, -done, done), 8)

        @pl.when(jnp.logical_and(turn >= 2, turn != 3))
        def _():
            unpack(zb)

            @pl.loop(0, 2)
            def _(i):
                use(zb, 1 - i)

                @pl.when(turn == 10)
                def _():
                    send_back(1 - i)

    for k in range(1, 8):
        idx = lax.rem(tp + k, 8)
        remote(pool_in.at[0], pool_in.at[idx], p_send.at[k], p_recv.at[idx], sib).wait_recv()
    for offset in (0, -1, 1, 2):
        weights_out.wait_sibling(offset)
    for t in range(8):
        lhs[:, pl.ds(t * 128, 128)] = pool_in[t]

    def out_part(first, part_of):
        columns = pl.ds(part_of * 512, 512)
        return dot(lhs[...], w_all[:, pl.ds(first, 128), columns].reshape(D // 2, 512)), columns

    for part_of in range(4):
        value, columns = out_part(0, part_of)
        total[:, columns] = value

    mine = jnp.logical_and(even, 2 * c == y)

    @pl.loop(0, 16)
    def _(head):
        @pl.when(jnp.logical_not(jnp.logical_and(mine, head == 4 * x + y)))
        def _():
            remote(att_all.at[0], att_all.at[head], o_send.at[0, 0], o_recv.at[head], sib).wait_recv()

    for t in range(8):
        two = [att_all[2 * t], att_all[2 * t + 1]]
        for h in range(2):
            rows = [value[:, h * 64 : h * 64 + 64] for value in two]
            lhs[pl.ds(h * HALF, HALF), pl.ds(t * 128, 128)] = jnp.concatenate(rows, axis=1)
    for part_of in range(4):
        value, columns = out_part(128, part_of)
        out_ref[:, columns] = (total[:, columns] + value).astype(BF16)

    acts.finish()
    kv_lats.finish()
    q_lats.finish()
    halo.wait_send()
    for j in range(2):
        @pl.when(jnp.logical_not(jnp.logical_and(even, 2 * c + j == y)))
        def _():
            q_copy(j).wait_send()

        @pl.when(2 * c + j != y)
        def _():
            kv_copy(j).wait_send()

    for qb in range(2):
        for t in range(8):
            @pl.when(jnp.logical_not(is_me(qb, t)))
            def _():
                back(qb, t).wait_send()

    for k in range(1, 8):
        pool_copy(k).wait_send()
    weights_out.finish()
    for b in range(2):
        for way in range(2):
            for s in range(4 if way == b else 3):
                ring_copy(0, way, b, s).wait_send()

    @pl.loop(0, 8)
    def _(zb):
        for b in range(2):
            sib_copy(zb * 4 + 2 * c + b).wait_send()


DMA = pltpu.SemaphoreType.DMA


def params(number):
    return pltpu.CompilerParams(collective_id=number, has_side_effects=True, vmem_limit_bytes=60 * 1024 * 1024)


def local(
    activations, in_gain, w_pool_in, pool_gain, w_qlat, w_kvlat, w_krope, qlat_gain, kvlat_gain,
    w_qup, w_kup, w_vup, qhead_gain, khead_gain, w_out_pool, w_out_attn,
):
    tables = [jnp.asarray(t) for t in rotary_tables()]
    gather_sems = [DMA((6,)), DMA((8,)), DMA((8, 2))]
    return pl.pallas_call(
        mixer_kernel,
        name="mixer",
        out_shape=jax.ShapeDtypeStruct((BLOCK, D), BF16),
        in_specs=[VMEM_SPEC] * 20,
        out_specs=VMEM_SPEC,
        scratch_shapes=[
            pltpu.VMEM((8, BLOCK, D), BF16),
            pltpu.VMEM((ROWS, 192), F32),
            pltpu.VMEM((64, ROWS), BF16),
            pltpu.VMEM((8, 64, ROWS), BF16),
            pltpu.VMEM((96, ROWS), BF16),
            pltpu.VMEM((8, 96, ROWS), BF16),
            pltpu.VMEM((HALO + ROWS, 128), F32),
            pltpu.VMEM((HALO, 128), BF16),
            pltpu.VMEM((HALO, 128), BF16),
            pltpu.VMEM((D, 192), BF16),
            pltpu.VMEM((256, KVLAT), BF16),
            pltpu.VMEM((2, HEAD, ROWS), BF16),
            pltpu.VMEM((2, LAT, ROWS), BF16),
            pltpu.VMEM((ROWS, 128), BF16),
            pltpu.VMEM((32, LAT, ROWS), BF16),
            pltpu.VMEM((32, ROWS, HEAD), BF16),
            pltpu.VMEM((2, HEAD, ROWS), BF16),
            pltpu.VMEM((2, VDIM, ROWS), F32),
            pltpu.VMEM((2, 8, ROWS), F32),
            pltpu.VMEM((2, 8, HALF, 128), BF16),
            pltpu.VMEM((16, HALF, 128), BF16),
            pltpu.VMEM((8, BLOCK, 128), BF16),
            pltpu.VMEM((8, 256, D), BF16),
            pltpu.VMEM((BLOCK, D // 2), BF16),
            pltpu.VMEM((BLOCK, D), F32),
            *gather_sems, *gather_sems, *gather_sems, DMA((2,)),
            DMA((2,)), DMA((32,)), DMA((2,)), DMA((2,)), DMA((2, 2, 4)), DMA((32,)), DMA((2, 8)), DMA((16,)),
            DMA((8,)), DMA((8,)), *gather_sems,
        ],
        compiler_params=params(1),
    )(
        activations, in_gain[None, :], w_pool_in, w_qlat.T, w_kvlat.T, w_krope.T, pool_gain[None, :], qlat_gain[None, :],
        kvlat_gain[None, :], w_qup.T, w_kup, w_vup, qhead_gain[None, :], khead_gain[None, :], *tables, w_out_pool, w_out_attn,
    )


def solution(mesh):
    placed = (
        P(("sp", "tp"), None), P(), P(None, "tp"), P("tp"), P(None, "tp"), P(None, "tp"), P(), P(), P(),
        P(None, "tp"), P(None, "tp"), P(None, "tp"), P(), P(), P("tp", None), P("tp", None),
    )
    return jax.shard_map(local, mesh=mesh, in_specs=placed, out_specs=P(("sp", "tp"), None), check_vma=False)
```

time: 128 us -> 124 us (0.969)
  the two profiles are of different devices: /device:TPU:111 before, /device:TPU:161 now
where the time goes in v3:
time: 124 us
  Pallas kernels  120 us (97%)
  local copies, waits for them, and re-layouts  3.03 us (2%)
    pallas_call x1, Pallas kernels, local(): pl.pallas_call(mixer_kernel, name='mixer', out_shape=jax.ShapeDtypeStruct...  120 us

profile of v3, /device:TPU:161, one launch (start us, length us, event | category | flops | bytes accessed | tf_op | source)
XLA Modules:
  0.0 123.5 jit_solution(10490406409946294399)
XLA Ops:
  0.0 0.0 copy-start
  0.0 0.7 copy-done
  0.7 0.6 broadcast_in_dim.20.q_gain
  1.3 120.5 %mixer.1 = bf16[96,2048]{1,0:T(8,128)(2,1)} custom-call(bf16[96,2048]{1,0:T(8,128)(2,1)} %act.1, f32[1,2048]{1,0:T(1,128)} %bitcast.13, bf16[2048,128]{1,0:T(8,128)(2,1)} %w_pool.1, bf16[96,2048]{1,0:T(8,128)(2,1)} %bitcast.9, bf16[64,2048]{1,0:T(8,128)(2,1)} %bitcast.11, bf16[32,2048]{1,0:T(8,128)(2,1)} %bitcast.12, f32[1,128]{1,0:T(1,128)} %bitcast.15, ...), custom_call_target="tpu_custom_call" | custom-call | tf_op jit(solution)/shard_map/mixer/pallas_call | solution.py:534
  121.8 1.8 %copy.22 = bf16[96,2048]{1,0:T(8,128)(2,1)} copy(bf16[96,2048]{1,0:T(8,128)(2,1)} %mixer.1) | data formatting | bytes 786432
Async XLA Ops:
  0.0 0.7 copy-start

commit v4 on v3

--- a/solution.py
+++ b/solution.py
@@ -141,9 +141,7 @@
     z, y = sp // 4, lax.rem(sp, 4)
     even = lax.rem(y, 2) == 0
     owner = y // 2
-    part = lax.rem(y, 2)
-    q_z = jnp.where(even, z, 7 - z)
-    q_c = jnp.where(even, owner, (3 - y) // 2)
+    q_c = jnp.where(y < 2, y, 3 - y)
 
     def device(yy, zz, cc, xx=x):
         return {"sp": zz * 4 + yy, "tp": xx * 2 + cc}
@@ -166,13 +164,12 @@
     for dy in range(4):
         for dc in range(2):
             yy, cc = lax.rem(y + dy, 4), lax.rem(c + dc, 2)
-            friends.append(device(yy, 7 - z, cc))
             if dy or dc:
                 friends.append(device(yy, z, cc))
     friends += [{"sp": sp, "tp": lax.rem(tp + k, 8)} for k in range(1, 8)]
     for dx in range(1, 4):
         for dy in range(4):
-            friends.append(device(lax.rem(y + dy, 4), q_z, q_c, lax.rem(x + dx, 4)))
+            friends.append(device(lax.rem(y + dy, 4), z, q_c, lax.rem(x + dx, 4)))
     meet(friends)
 
     acts.start()
@@ -247,7 +244,7 @@
         return remote(kv_own.at[j], kv_all.at[sp], c_send.at[j], kv_recv.at[sp], device(2 * c + j, z, owner))
 
     def q_copy(j):
-        return remote(q_own.at[j], q_in.at[part], q_send.at[j], q_recv.at[part], device(2 * c + j, q_z, q_c))
+        return remote(q_own.at[j], q_in.at[owner], q_send.at[j], q_recv.at[owner], device(2 * c + j, z, q_c))
 
     for j in range(2):
         here = 2 * c + j == y
@@ -281,7 +278,7 @@
 
         @pl.when(here)
         def _():
-            q_in[0] = q_own[j]
+            q_in[owner] = q_own[j]
 
     def wait_slot(slot):
         remote(kv_all.at[slot], kv_all.at[slot], sib_send.at[slot], kv_recv.at[slot], sib).wait_recv()
@@ -317,18 +314,26 @@
         den[...] = jnp.zeros_like(den)
 
     def attend(slots, qb, diagonal):
-        for qc in range(3):
+        units = [(slot, qc) for slot in slots for qc in range(3)]
+
+        def score(unit):
+            slot, qc = unit
+            keys = (qc + 1) * 256 if diagonal else ROWS
+            return dot(k_rows[slot, pl.ds(0, keys), :], q_in[qb, :, pl.ds(qc * 256, 256)])
+
+        ready = [score(unit) for unit in units[:2]]
+        for i, (slot, qc) in enumerate(units):
+            if i + 2 < len(units):
+                ready.append(score(units[i + 2]))
             columns = pl.ds(qc * 256, 256)
             keys = (qc + 1) * 256 if diagonal else ROWS
-            for slot in slots:
-                scores = dot(k_rows[slot, pl.ds(0, keys), :], q_in[qb, :, columns])
-                weights = jnp.exp2(scores)
-                if diagonal:
-                    k_pos = lax.broadcasted_iota(jnp.int32, (keys, 256), 0)
-                    q_pos = lax.broadcasted_iota(jnp.int32, (keys, 256), 1) + qc * 256
-                    weights = jnp.where(k_pos <= q_pos, weights, 0.0)
-                den[qb, :, columns] += jnp.sum(weights.reshape(keys // 8, 8, 256), axis=0)
-                acc[qb, :, columns] += dot(kv_all[slot, pl.ds(96, 64), pl.ds(0, keys)], weights.astype(BF16))
+            weights = jnp.exp2(ready.pop(0))
+            if diagonal:
+                k_pos = lax.broadcasted_iota(jnp.int32, (keys, 256), 0)
+                q_pos = lax.broadcasted_iota(jnp.int32, (keys, 256), 1) + qc * 256
+                weights = jnp.where(k_pos <= q_pos, weights, 0.0)
+            den[qb, :, columns] += jnp.sum(weights.reshape(keys // 8, 8, 256), axis=0)
+            acc[qb, :, columns] += dot(kv_all[slot, pl.ds(96, 64), pl.ds(0, keys)], weights.astype(BF16))
 
     def plane_of(way, s):
         return lax.rem(z + 8 - s, 8) if way == 0 else lax.rem(z + s, 8)
@@ -354,28 +359,28 @@
             def _():
                 sib_copy(slot).start()
 
-    def query_block(qb):
-        return jnp.where(qb == 0, z, 7 - z), jnp.where(qb == 0, 2 * c, 3 - 2 * c)
+    def query_row(qb):
+        return jnp.where(qb == 0, c, 3 - c)
 
     def unpack(zb):
         first = zb * 4
         for b in range(2):
             wait_slot(first + 2 * (1 - c) + b)
 
-        @pl.when(zb <= jnp.maximum(z, 7 - z))
+        @pl.when(zb <= z)
         def _():
             for yb in range(4):
                 k_rows[first + yb] = turned(kv_all[first + yb, pl.ds(0, HEAD), :]).astype(BF16)
 
     def use(zb, qb):
         first = zb * 4
-        plane, row = query_block(qb)
-
-        @pl.when(zb < plane)
+        row = query_row(qb)
+
+        @pl.when(zb < z)
         def _():
             attend([first + yb for yb in range(4)], qb, False)
 
-        @pl.when(zb == plane)
+        @pl.when(zb == z)
         def _():
             @pl.loop(0, row)
             def _(yb):
@@ -384,14 +389,13 @@
             attend([first + row], qb, True)
 
     def back(qb, t):
-        to_z, to_y = query_block(qb)
         return remote(
             o_rows.at[qb, t], att_all.at[4 * x + y], o_send.at[qb, t], o_recv.at[4 * x + y],
-            {"sp": to_z * 4 + to_y, "tp": t},
+            {"sp": z * 4 + query_row(qb), "tp": t},
         )
 
     def is_me(qb, t):
-        return jnp.logical_and(jnp.logical_and(qb == 0, 2 * c == y), tp == t)
+        return jnp.logical_and(query_row(qb) == y, tp == t)
 
     def send_back(qb):
         rows = jnp.transpose(acc[qb] / jnp.sum(den[qb], axis=0, keepdims=True)).reshape(8, 2, HALF, VDIM)
@@ -417,13 +421,12 @@
         def _():
             mix_pool()
 
-        @pl.when(jnp.logical_and(turn == 1, 2 * c != y))
-        def _():
-            remote(q_own.at[0], q_in.at[0], q_send.at[0], q_recv.at[0], sib).wait_recv()
-
-        @pl.when(turn == 1)
-        def _():
-            remote(q_own.at[0], q_in.at[1], q_send.at[0], q_recv.at[1], sib).wait_recv()
+        for qb in range(2):
+            kept = jnp.logical_and(jnp.logical_and(even, 2 * c == y), owner == qb)
+
+            @pl.when(jnp.logical_and(turn == 1, jnp.logical_not(kept)))
+            def _():
+                remote(q_own.at[0], q_in.at[qb], q_send.at[0], q_recv.at[qb], sib).wait_recv()
 
         @pl.when(turn == 4)
         def _():
@@ -468,7 +471,7 @@
         value, columns = out_part(0, part_of)
         total[:, columns] = value
 
-    mine = jnp.logical_and(even, 2 * c == y)
+    mine = q_c == c
 
     @pl.loop(0, 16)
     def _(head):

time: 124 us -> 108 us (0.87)
  the two profiles are of different devices: /device:TPU:161 before, /device:TPU:225 now
where the time goes in v4:
time: 108 us
  Pallas kernels  105 us (97%)
  local copies, waits for them, and re-layouts  3.03 us (3%)
    pallas_call x1, Pallas kernels, local(): pl.pallas_call(mixer_kernel, name='mixer', out_shape=jax.ShapeDtypeStruct...  105 us
    unnamed x3, local copies, waits for them, and re-layouts  2.45 us

profile of v4, /device:TPU:225, one launch (start us, length us, event | category | flops | bytes accessed | tf_op | source)
XLA Modules:
  0.0 107.6 jit_solution(18295062558147939153)
XLA Ops:
  0.0 0.0 copy-start
  0.0 0.7 copy-done
  0.7 0.6 broadcast_in_dim.20.q_gain
  1.3 104.6 %mixer.1 = bf16[96,2048]{1,0:T(8,128)(2,1)} custom-call(bf16[96,2048]{1,0:T(8,128)(2,1)} %act.1, f32[1,2048]{1,0:T(1,128)} %bitcast.13, bf16[2048,128]{1,0:T(8,128)(2,1)} %w_pool.1, bf16[96,2048]{1,0:T(8,128)(2,1)} %bitcast.9, bf16[64,2048]{1,0:T(8,128)(2,1)} %bitcast.11, bf16[32,2048]{1,0:T(8,128)(2,1)} %bitcast.12, f32[1,128]{1,0:T(1,128)} %bitcast.15, ...), custom_call_target="tpu_custom_call" | custom-call | tf_op jit(solution)/shard_map/mixer/pallas_call | solution.py:537
  105.8 1.8 %copy.22 = bf16[96,2048]{1,0:T(8,128)(2,1)} copy(bf16[96,2048]{1,0:T(8,128)(2,1)} %mixer.1) | data formatting | bytes 786432
Async XLA Ops:
  0.0 0.7 copy-start

commit v5 on v4

--- a/solution.py
+++ b/solution.py
@@ -257,38 +257,6 @@
         def _():
             kv_all[sp] = kv_own[j]
 
-    q_lats.relay_first()
-    q_lats.relay_second()
-    q_lats.relay_far()
-    for offset in (0, -1, 1, 2):
-        q_lats.wait_sibling(offset)
-    weights_out.start()
-    q_lat = ql_all[...].reshape(QLAT, ROWS).astype(F32)
-    q_norm = q_lat * lax.rsqrt(jnp.sum(q_lat * q_lat, axis=0, keepdims=True) / QLAT + EPS) * column(q_gain)
-    raw = dot(wq_t[...], q_norm.astype(BF16)).astype(BF16).astype(F32)
-    for h in range(2):
-        q_own[h] = (finish(raw[h * 96 : h * 96 + 96], column(qh_gain)) * SCALE).astype(BF16)
-
-    for j in range(2):
-        here = jnp.logical_and(even, 2 * c + j == y)
-
-        @pl.when(jnp.logical_not(here))
-        def _():
-            q_copy(j).start()
-
-        @pl.when(here)
-        def _():
-            q_in[owner] = q_own[j]
-
-    def wait_slot(slot):
-        remote(kv_all.at[slot], kv_all.at[slot], sib_send.at[slot], kv_recv.at[slot], sib).wait_recv()
-
-    def ring_copy(slot, way, b, s):
-        return remote(kv_all.at[slot], kv_all.at[slot], ring_send.at[way, b, s], kv_recv.at[slot], (up, down)[way])
-
-    def sib_copy(slot):
-        return remote(kv_all.at[slot], kv_all.at[slot], sib_send.at[slot], kv_recv.at[slot], sib)
-
     def pool_copy(k):
         to = lax.rem(tp + k, 8)
         rows = pl.multiple_of(to * BLOCK, 32)
@@ -313,16 +281,49 @@
         acc[...] = jnp.zeros_like(acc)
         den[...] = jnp.zeros_like(den)
 
-    def attend(slots, qb, diagonal):
-        units = [(slot, qc) for slot in slots for qc in range(3)]
+    q_lats.relay_first()
+    q_lats.relay_second()
+    mix_pool()
+    q_lats.relay_far()
+    for offset in (0, -1, 1, 2):
+        q_lats.wait_sibling(offset)
+    weights_out.start()
+    q_lat = ql_all[...].reshape(QLAT, ROWS).astype(F32)
+    q_norm = q_lat * lax.rsqrt(jnp.sum(q_lat * q_lat, axis=0, keepdims=True) / QLAT + EPS) * column(q_gain)
+    raw = dot(wq_t[...], q_norm.astype(BF16)).astype(BF16).astype(F32)
+    for h in range(2):
+        q_own[h] = (finish(raw[h * 96 : h * 96 + 96], column(qh_gain)) * SCALE).astype(BF16)
+
+    for j in range(2):
+        here = jnp.logical_and(even, 2 * c + j == y)
+
+        @pl.when(jnp.logical_not(here))
+        def _():
+            q_copy(j).start()
+
+        @pl.when(here)
+        def _():
+            q_in[owner] = q_own[j]
+
+    def wait_slot(slot):
+        remote(kv_all.at[slot], kv_all.at[slot], sib_send.at[slot], kv_recv.at[slot], sib).wait_recv()
+
+    def ring_copy(slot, way, b, s):
+        return remote(kv_all.at[slot], kv_all.at[slot], ring_send.at[way, b, s], kv_recv.at[slot], (up, down)[way])
+
+    def sib_copy(slot):
+        return remote(kv_all.at[slot], kv_all.at[slot], sib_send.at[slot], kv_recv.at[slot], sib)
+
+    def attend(slots, blocks, diagonal):
+        units = [(slot, qb, qc) for slot in slots for qb in blocks for qc in range(3)]
 
         def score(unit):
-            slot, qc = unit
+            slot, qb, qc = unit
             keys = (qc + 1) * 256 if diagonal else ROWS
             return dot(k_rows[slot, pl.ds(0, keys), :], q_in[qb, :, pl.ds(qc * 256, 256)])
 
         ready = [score(unit) for unit in units[:2]]
-        for i, (slot, qc) in enumerate(units):
+        for i, (slot, qb, qc) in enumerate(units):
             if i + 2 < len(units):
                 ready.append(score(units[i + 2]))
             columns = pl.ds(qc * 256, 256)
@@ -362,31 +363,34 @@
     def query_row(qb):
         return jnp.where(qb == 0, c, 3 - c)
 
-    def unpack(zb):
-        first = zb * 4
+    def turn_keys(slot):
+        k_rows[slot] = turned(kv_all[slot, pl.ds(0, HEAD), :]).astype(BF16)
+
+    def use_own_plane():
         for b in range(2):
-            wait_slot(first + 2 * (1 - c) + b)
-
-        @pl.when(zb <= z)
-        def _():
-            for yb in range(4):
-                k_rows[first + yb] = turned(kv_all[first + yb, pl.ds(0, HEAD), :]).astype(BF16)
-
-    def use(zb, qb):
-        first = zb * 4
-        row = query_row(qb)
-
-        @pl.when(zb < z)
-        def _():
-            attend([first + yb for yb in range(4)], qb, False)
-
-        @pl.when(zb == z)
-        def _():
+            wait_slot(z * 4 + 2 * (1 - c) + b)
+        for yb in range(4):
+            turn_keys(z * 4 + yb)
+
+        @pl.loop(0, 2)
+        def _(qb):
+            row = query_row(qb)
+
             @pl.loop(0, row)
             def _(yb):
-                attend([first + yb], qb, False)
-
-            attend([first + row], qb, True)
+                attend([z * 4 + yb], [qb], False)
+
+            attend([z * 4 + row], [qb], True)
+
+    def use_pair(zb, b):
+        wait_slot(zb * 4 + 2 * (1 - c) + b)
+
+        @pl.when(zb < z)
+        def _():
+            pair = [zb * 4 + b, zb * 4 + 2 + b]
+            for slot in pair:
+                turn_keys(slot)
+            attend(pair, (0, 1), False)
 
     def back(qb, t):
         return remote(
@@ -417,10 +421,6 @@
             def _():
                 pass_on(s, k)
 
-        @pl.when(turn == 1)
-        def _():
-            mix_pool()
-
         for qb in range(2):
             kept = jnp.logical_and(jnp.logical_and(even, 2 * c == y), owner == qb)
 
@@ -440,20 +440,20 @@
         def _():
             weights_out.relay_far()
 
-        done = s - 1
-        zb = lax.rem(z + 8 + jnp.where(b == 0, -done, done), 8)
-
-        @pl.when(jnp.logical_and(turn >= 2, turn != 3))
-        def _():
-            unpack(zb)
-
-            @pl.loop(0, 2)
-            def _(i):
-                use(zb, 1 - i)
-
-                @pl.when(turn == 10)
-                def _():
-                    send_back(1 - i)
+        @pl.when(turn == 1)
+        def _():
+            use_own_plane()
+
+        step, half = (turn - 1) // 2, lax.rem(turn + 1, 2)
+
+        @pl.when(turn >= 3)
+        def _():
+            @pl.loop(0, jnp.where(step < 4, 2, 1))
+            def _(side):
+                use_pair(lax.rem(z + 8 + jnp.where(side == 0, -step, step), 8), half)
+
+    for qb in range(2):
+        send_back(qb)
 
     for k in range(1, 8):
         idx = lax.rem(tp + k, 8)

time: 108 us -> 102 us (0.944)
  Pallas kernels: 105 us -> 99.2 us
    pallas_call x1, Pallas kernels: 105 us -> 99.2 us  [local(): pl.pallas_call(mixer_kernel, name='mixer', out_shape=jax.ShapeDtypeStruct...]
where the time goes in v5:
time: 102 us
  Pallas kernels  99.2 us (97%)
  local copies, waits for them, and re-layouts  3.03 us (3%)
    pallas_call x1, Pallas kernels, local(): pl.pallas_call(mixer_kernel, name='mixer', out_shape=jax.ShapeDtypeStruct...  99.2 us
    unnamed x3, local copies, waits for them, and re-layouts  2.45 us

profile of v5, /device:TPU:225, one launch (start us, length us, event | category | flops | bytes accessed | tf_op | source)
XLA Modules:
  0.0 102.3 jit_solution(3069336894207515011)
XLA Ops:
  0.0 0.0 copy-start
  0.0 0.7 copy-done
  0.7 0.6 broadcast_in_dim.20.q_gain
  1.3 99.2 %mixer.1 = bf16[96,2048]{1,0:T(8,128)(2,1)} custom-call(bf16[96,2048]{1,0:T(8,128)(2,1)} %act.1, f32[1,2048]{1,0:T(1,128)} %bitcast.13, bf16[2048,128]{1,0:T(8,128)(2,1)} %w_pool.1, bf16[96,2048]{1,0:T(8,128)(2,1)} %bitcast.9, bf16[64,2048]{1,0:T(8,128)(2,1)} %bitcast.11, bf16[32,2048]{1,0:T(8,128)(2,1)} %bitcast.12, f32[1,128]{1,0:T(1,128)} %bitcast.15, ...), custom_call_target="tpu_custom_call" | custom-call | tf_op jit(solution)/shard_map/mixer/pallas_call | solution.py:537
  100.5 1.8 %copy.22 = bf16[96,2048]{1,0:T(8,128)(2,1)} copy(bf16[96,2048]{1,0:T(8,128)(2,1)} %mixer.1) | data formatting | bytes 786432
Async XLA Ops:
  0.0 0.7 copy-start

commit v6 on v5

--- a/solution.py
+++ b/solution.py
@@ -27,6 +27,7 @@
 BF16 = jnp.bfloat16
 MESH = pl.DeviceIdType.MESH
 VMEM_SPEC = pl.BlockSpec(memory_space=pltpu.VMEM)
+ANY_SPEC = pl.BlockSpec(memory_space=pl.ANY)
 SCALE = (1.0 / math.sqrt(HEAD)) * math.log2(math.e)
 
 
@@ -38,8 +39,9 @@
     return jnp.transpose(a.astype(F32))
 
 
-def column(row_ref):
-    return jnp.transpose(jnp.broadcast_to(row_ref[...], (8, row_ref.shape[1])))[:, 0:1]
+def column(gain, flat=False):
+    row = gain[...][None, :] if flat else gain[...]
+    return jnp.transpose(jnp.broadcast_to(row, (8, row.shape[1])))[:, 0:1]
 
 
 def rotary_tables():
@@ -129,9 +131,10 @@
 
 
 def mixer_kernel(
-    act, in_gain, w_pool, w_qlat_t, w_kvlat_t, w_krope_t, pool_gain, q_gain, kv_gain, wq_t, w_kup, w_vup, qh_gain, kh_gain,
+    act, in_gain, w_pool_hbm, w_qlat_hbm, w_kvlat_hbm, w_krope_hbm, pool_gain, q_gain, kv_gain, wq_hbm, w_kup_hbm, w_vup_hbm, qh_gain, kh_gain,
     far_cos, far_sin, near_cos, near_sin, w_out_pool, w_out_attn,
     out_ref,
+    w_pool, w_lat_t, wq_t, w_up, load_sem,
     act_all, lat_rows, kvl_own, kvl_all, ql_own, ql_all, pool_rows, halo_out, halo_in, w_lat, wkv_t, q_own, kv_own, pool_own,
     kv_all, k_rows, q_in, acc, den, o_rows, att_all, pool_in, w_all, lhs, total,
     a_ring, a_sib, a_recv, k_ring, k_sib, k_recv, l_ring, l_sib, l_recv, halo_sem,
@@ -155,10 +158,21 @@
     def gather(own, everything, half, *sems):
         return TpGather(own, everything, half, sp, x, c, *sems)
 
+    loads = [
+        pltpu.make_async_copy(src, dst, load_sem.at[k])
+        for k, (src, dst) in enumerate((
+            (w_qlat_hbm, w_lat_t.at[pl.ds(0, 96)]), (w_kvlat_hbm, w_lat_t.at[pl.ds(96, 64)]), (w_krope_hbm, w_lat_t.at[pl.ds(160, 32)]),
+            (w_pool_hbm, w_pool), (w_kup_hbm, w_up.at[0]), (w_vup_hbm, w_up.at[1]), (wq_hbm, wq_t),
+            (w_out_pool, w_all.at[tp, pl.ds(0, 128)]), (w_out_attn, w_all.at[tp, pl.ds(128, 128)]),
+        ))
+    ]
+    for load in loads:
+        load.start()
+
     acts = gather([act.at[pl.ds(0, HALF)], act.at[pl.ds(HALF, HALF)]], act_all, HALF, a_ring, a_sib, a_recv)
     kv_lats = gather([kvl_own.at[pl.ds(0, 32)], kvl_own.at[pl.ds(32, 32)]], kvl_all, 32, k_ring, k_sib, k_recv)
     q_lats = gather([ql_own.at[pl.ds(0, 48)], ql_own.at[pl.ds(48, 48)]], ql_all, 48, l_ring, l_sib, l_recv)
-    weights_out = gather([w_out_pool, w_out_attn], w_all, 128, w_ring, w_sib, w_recv)
+    weights_out = gather([w_all.at[tp, pl.ds(0, 128)], w_all.at[tp, pl.ds(128, 128)]], w_all, 128, w_ring, w_sib, w_recv)
 
     friends = [up, down, behind, before]
     for dy in range(4):
@@ -182,10 +196,12 @@
         pool_rows[pl.ds(HALO + rows, BLOCK), :] = dot(normed, w_pool[...]).astype(BF16).astype(F32)
         lat_rows[pl.ds(rows, BLOCK), :] = dot(normed, w_lat[...])
 
-    w_lat[...] = turned(jnp.concatenate([w_qlat_t[...], w_kvlat_t[...], w_krope_t[...]], axis=0)).astype(BF16)
+    for load in loads:
+        load.wait()
+    w_lat[...] = turned(w_lat_t[...]).astype(BF16)
     project(act, tp)
-    wkv_t[pl.ds(0, 128), :] = turned(w_kup[...]).astype(BF16)
-    wkv_t[pl.ds(128, 128), :] = turned(w_vup[...]).astype(BF16)
+    wkv_t[pl.ds(0, 128), :] = turned(w_up[0]).astype(BF16)
+    wkv_t[pl.ds(128, 128), :] = turned(w_up[1]).astype(BF16)
     idx = acts.wait_sibling(0)
     project(act_all.at[idx], idx)
     acts.relay_first()
@@ -276,8 +292,6 @@
         for k in range(1, 8):
             pool_copy(k).start()
         pool_in[tp] = pool_own[pl.ds(pl.multiple_of(tp * BLOCK, 32), BLOCK), :]
-        w_all[tp, pl.ds(0, 128), :] = w_out_pool[...]
-        w_all[tp, pl.ds(128, 128), :] = w_out_attn[...]
         acc[...] = jnp.zeros_like(acc)
         den[...] = jnp.zeros_like(den)
 
@@ -288,22 +302,23 @@
     for offset in (0, -1, 1, 2):
         q_lats.wait_sibling(offset)
     weights_out.start()
-    q_lat = ql_all[...].reshape(QLAT, ROWS).astype(F32)
-    q_norm = q_lat * lax.rsqrt(jnp.sum(q_lat * q_lat, axis=0, keepdims=True) / QLAT + EPS) * column(q_gain)
-    raw = dot(wq_t[...], q_norm.astype(BF16)).astype(BF16).astype(F32)
-    for h in range(2):
-        q_own[h] = (finish(raw[h * 96 : h * 96 + 96], column(qh_gain)) * SCALE).astype(BF16)
-
-    for j in range(2):
-        here = jnp.logical_and(even, 2 * c + j == y)
-
-        @pl.when(jnp.logical_not(here))
-        def _():
-            q_copy(j).start()
-
-        @pl.when(here)
-        def _():
-            q_in[owner] = q_own[j]
+    def ask():
+        q_lat = ql_all[...].reshape(QLAT, ROWS).astype(F32)
+        q_norm = q_lat * lax.rsqrt(jnp.sum(q_lat * q_lat, axis=0, keepdims=True) / QLAT + EPS) * column(q_gain, True)
+        raw = dot(wq_t[...], q_norm.astype(BF16)).astype(BF16).astype(F32)
+        for h in range(2):
+            q_own[h] = (finish(raw[h * 96 : h * 96 + 96], column(qh_gain)) * SCALE).astype(BF16)
+
+        for j in range(2):
+            here = jnp.logical_and(even, 2 * c + j == y)
+
+            @pl.when(jnp.logical_not(here))
+            def _():
+                q_copy(j).start()
+
+            @pl.when(here)
+            def _():
+                q_in[owner] = q_own[j]
 
     def wait_slot(slot):
         remote(kv_all.at[slot], kv_all.at[slot], sib_send.at[slot], kv_recv.at[slot], sib).wait_recv()
@@ -421,6 +436,10 @@
             def _():
                 pass_on(s, k)
 
+        @pl.when(turn == 1)
+        def _():
+            ask()
+
         for qb in range(2):
             kept = jnp.logical_and(jnp.logical_and(even, 2 * c == y), owner == qb)
 
@@ -538,9 +557,14 @@
         mixer_kernel,
         name="mixer",
         out_shape=jax.ShapeDtypeStruct((BLOCK, D), BF16),
-        in_specs=[VMEM_SPEC] * 20,
+        in_specs=[ANY_SPEC if k in (2, 3, 4, 5, 9, 10, 11, 18, 19) else VMEM_SPEC for k in range(20)],
         out_specs=VMEM_SPEC,
         scratch_shapes=[
+            pltpu.VMEM((D, 128), BF16),
+            pltpu.VMEM((192, D), BF16),
+            pltpu.VMEM((192, QLAT), BF16),
+            pltpu.VMEM((2, KVLAT, 128), BF16),
+            DMA((9,)),
             pltpu.VMEM((8, BLOCK, D), BF16),
             pltpu.VMEM((ROWS, 192), F32),
             pltpu.VMEM((64, ROWS), BF16),
@@ -572,7 +596,7 @@
         ],
         compiler_params=params(1),
     )(
-        activations, in_gain[None, :], w_pool_in, w_qlat.T, w_kvlat.T, w_krope.T, pool_gain[None, :], qlat_gain[None, :],
+        activations, in_gain[None, :], w_pool_in, w_qlat.T, w_kvlat.T, w_krope.T, pool_gain[None, :], qlat_gain,
         kvlat_gain[None, :], w_qup.T, w_kup, w_vup, qhead_gain[None, :], khead_gain[None, :], *tables, w_out_pool, w_out_attn,
     )
 

time: 102 us -> 100 us (0.980)
  Pallas kernels: 99.2 us -> 97.8 us
  local copies, waits for them, and re-layouts: 3.03 us -> 1.77 us
    pallas_call x1, Pallas kernels: 99.2 us -> 97.8 us  [local(): pl.pallas_call(mixer_kernel, name='mixer', out_shape=jax.ShapeDtypeStruct...]
    unnamed x3 -> x1, local copies, waits for them, and re-layouts: 2.45 us -> 1.77 us
where the time goes in v6:
time: 100 us; the launch traced here: 99.6 us
  Pallas kernels  97.8 us (98%)
  local copies, waits for them, and re-layouts  1.77 us (2%)
    pallas_call x1, Pallas kernels, local(): pl.pallas_call(mixer_kernel, name='mixer', out_shape=jax.ShapeDtypeStruct...  97.8 us

profile of v6, /device:TPU:225, one launch (start us, length us, event | category | flops | bytes accessed | tf_op | source)
XLA Modules:
  0.0 99.6 jit_solution(681505827589987718)
XLA Ops:
  0.0 97.8 %mixer.1 = bf16[96,2048]{1,0:T(8,128)(2,1)} custom-call(bf16[96,2048]{1,0:T(8,128)(2,1)} %act.1, f32[1,2048]{1,0:T(1,128)} %bitcast.13, bf16[2048,128]{1,0:T(8,128)(2,1)} %w_pool_hbm.1, bf16[96,2048]{1,0:T(8,128)(2,1)} %bitcast.9, bf16[64,2048]{1,0:T(8,128)(2,1)} %bitcast.11, bf16[32,2048]{1,0:T(8,128)(2,1)} %bitcast.12, f32[1,128]{1,0:T(1,128)} %bitcast.15, ...), custom_call_target="tpu_custom_call" | custom-call | tf_op jit(solution)/shard_map/mixer/pallas_call | solution.py:556
  97.8 1.8 %copy.22 = bf16[96,2048]{1,0:T(8,128)(2,1)} copy(bf16[96,2048]{1,0:T(8,128)(2,1)} %mixer.1) | data formatting | bytes 786432

commit v7 on v6

--- a/solution.py
+++ b/solution.py
@@ -431,38 +431,6 @@
     @pl.loop(0, 11)
     def _(turn):
         s, b = turn // 2, lax.rem(turn, 2)
-        for k in range(2):
-            @pl.when(jnp.logical_and(b == k, turn < 10))
-            def _():
-                pass_on(s, k)
-
-        @pl.when(turn == 1)
-        def _():
-            ask()
-
-        for qb in range(2):
-            kept = jnp.logical_and(jnp.logical_and(even, 2 * c == y), owner == qb)
-
-            @pl.when(jnp.logical_and(turn == 1, jnp.logical_not(kept)))
-            def _():
-                remote(q_own.at[0], q_in.at[qb], q_send.at[0], q_recv.at[qb], sib).wait_recv()
-
-        @pl.when(turn == 4)
-        def _():
-            weights_out.relay_first()
-
-        @pl.when(turn == 6)
-        def _():
-            weights_out.relay_second()
-
-        @pl.when(turn == 8)
-        def _():
-            weights_out.relay_far()
-
-        @pl.when(turn == 1)
-        def _():
-            use_own_plane()
-
         step, half = (turn - 1) // 2, lax.rem(turn + 1, 2)
 
         @pl.when(turn >= 3)
@@ -470,6 +438,42 @@
             @pl.loop(0, jnp.where(step < 4, 2, 1))
             def _(side):
                 use_pair(lax.rem(z + 8 + jnp.where(side == 0, -step, step), 8), half)
+
+        for k in range(2):
+            @pl.when(jnp.logical_and(b == k, turn < 9))
+            def _():
+                pass_on(s, k)
+
+        @pl.when(turn == 1)
+        def _():
+            ask()
+
+        for qb in range(2):
+            kept = jnp.logical_and(jnp.logical_and(even, 2 * c == y), owner == qb)
+
+            @pl.when(jnp.logical_and(turn == 1, jnp.logical_not(kept)))
+            def _():
+                remote(q_own.at[0], q_in.at[qb], q_send.at[0], q_recv.at[qb], sib).wait_recv()
+
+        @pl.when(turn == 4)
+        def _():
+            weights_out.relay_first()
+
+        @pl.when(turn == 6)
+        def _():
+            weights_out.relay_second()
+
+        @pl.when(turn == 8)
+        def _():
+            weights_out.relay_far()
+
+        @pl.when(turn == 1)
+        def _():
+            use_own_plane()
+
+        @pl.when(turn == 8)
+        def _():
+            pass_on(s, 1)
 
     for qb in range(2):
         send_back(qb)

time: 100 us -> 104 us (1.040)
  Pallas kernels: 97.8 us -> 101 us
    pallas_call x1, Pallas kernels: 97.8 us -> 101 us  [local(): pl.pallas_call(mixer_kernel, name='mixer', out_shape=jax.ShapeDtypeStruct...]
where the time goes in v7:
time: 104 us; the launch traced here: 103 us
  Pallas kernels  101 us (97%)
  local copies, waits for them, and re-layouts  1.77 us (2%)
    pallas_call x1, Pallas kernels, local(): pl.pallas_call(mixer_kernel, name='mixer', out_shape=jax.ShapeDtypeStruct...  101 us

profile of v7, /device:TPU:225, one launch (start us, length us, event | category | flops | bytes accessed | tf_op | source)
XLA Modules:
  0.0 103.1 jit_solution(13477487520634583754)
XLA Ops:
  0.0 101.3 %mixer.1 = bf16[96,2048]{1,0:T(8,128)(2,1)} custom-call(bf16[96,2048]{1,0:T(8,128)(2,1)} %act.1, f32[1,2048]{1,0:T(1,128)} %bitcast.13, bf16[2048,128]{1,0:T(8,128)(2,1)} %w_pool_hbm.1, bf16[96,2048]{1,0:T(8,128)(2,1)} %bitcast.9, bf16[64,2048]{1,0:T(8,128)(2,1)} %bitcast.11, bf16[32,2048]{1,0:T(8,128)(2,1)} %bitcast.12, f32[1,128]{1,0:T(1,128)} %bitcast.15, ...), custom_call_target="tpu_custom_call" | custom-call | tf_op jit(solution)/shard_map/mixer/pallas_call | solution.py:560
  101.4 1.8 %copy.22 = bf16[96,2048]{1,0:T(8,128)(2,1)} copy(bf16[96,2048]{1,0:T(8,128)(2,1)} %mixer.1) | data formatting | bytes 786432
